TPU v7x, 128 devices: a whole 4x4x4 slice. The times are simulated.
128 devices in a mesh: sp: 16 (over z, x), tp: 8 (over y, core).
Axes of the slice: x: 4, y: 4, z: 4, core: 2. Of those that a mesh axis runs over, the one named last changes fastest.
Arguments:
- x_in: bfloat16 [16, 6144, 2048], P('tp', 'sp'), may hold values from -13 to 13
- x_new: bfloat16 [16, 2048], P('sp'), may hold values from -6 to 6
- w_x: bfloat16 [2048, 2048], replicated, may hold values from -0.125 to 0.125
- w_b: bfloat16 [2048, 1024], replicated, may hold values from -0.125 to 0.125
- w_c: bfloat16 [2048, 1024], replicated, may hold values from -0.125 to 0.125
- w_dt: bfloat16 [2048, 32], replicated, may hold values from -0.125 to 0.125
- w_z: bfloat16 [2048, 2048], P(None, 'tp'), may hold values from -3 to 3
- conv_w: float32 [4, 4096], replicated, may hold values from -3 to 3
- conv_b: float32 [4096], replicated, may hold values from -3 to 3
- dt_bias: float32 [32], replicated, may hold values from -4 to -2
- a_log: float32 [32], replicated, may hold values from -12 to 0
- d_skip: float32 [32], replicated, may hold values from 1 to 8
- norm_g: float32 [32, 64], P('tp'), may hold values from 0.1 to 1.9
Outputs:
- state_cache: bfloat16 [16, 32, 64, 128], P('sp', 'tp')
- read_out: bfloat16 [16, 32, 64], P('sp', 'tp')
All inputs are finite; a program needn't handle non-finite values.
Results may differ from a plain program's by a relative error of at most 0.015.
Values may be sent and summed in bfloat16 or wider, within the bound.
A program may use at most 128 MiB of HBM per device.

v0:
```python
import jax
import jax.numpy as jnp
from jax import lax
from jax.sharding import Mesh
from jax.sharding import PartitionSpec as P

H = 32
P_SIZE = 64
G = 8
N = 128
KW = 4
R = 4
TP = ("tp_0", "tp_1")


eps = 1e-05


def copy_for_each(value, axis):
    copies = jnp.broadcast_to(value, (lax.axis_size(axis), *value.shape))
    return lax.all_to_all(copies, axis, split_axis=0, concat_axis=0, tiled=True)


def combined_pairwise(pieces, combine):
    while len(jax.tree.leaves(pieces)[0]) > 1:
        pieces = jax.vmap(combine)(*(pieces[side::2] for side in (0, 1)))
    return pieces[0]


def prefix(value, axis, combine, identity):
    devices, index = (lax.axis_size(axis), lax.axis_index(axis))
    passed = jnp.arange(devices) > index

    def kept(part, zero, own):
        part = jnp.where(
            passed.reshape(-1, *(1 for _ in own.shape)), part, jnp.asarray(zero, own.dtype)
        )
        return part[::-1]

    pieces = copy_for_each(value, axis)
    return combined_pairwise(kept(pieces, identity, value), combine)


def passed_along(value, axis, steps):
    count = lax.axis_size(axis)
    first, last = (max(0, -steps), min(count, count - steps))
    return lax.ppermute(value, axis, [(source, source + steps) for source in range(first, last)])


def broadcast(value, axis, root):
    return lax.dynamic_index_in_dim(lax.all_gather(value, axis), root, 0, keepdims=False)


def joined_along(pieces, dim):
    pieces = jnp.moveaxis(pieces, 0, dim)
    dims = pieces.shape
    return pieces.reshape(*dims[:dim], dims[dim] * dims[dim + 1], *dims[dim + 2 :])


def all_blocks(value, axes, sequence):
    pieces = value[None]
    for k in sequence:
        pieces = lax.all_gather(pieces, axes[k], axis=0, tiled=True)
    held = [lax.axis_size(axes[k]) for k in reversed(sequence)]
    pieces = pieces.reshape(*held, *value.shape)
    turned = sorted(range(len(sequence)), key=lambda place: sequence[len(sequence) - 1 - place])
    return pieces.transpose(*turned, *range(len(sequence), pieces.ndim)).reshape(-1, *value.shape)


def gather_axes(value, axes, sequence, dim):
    return joined_along(all_blocks(value, axes, sequence), dim)


def in_blocks(value, dim, devices):
    before, after = (value.shape[:dim], value.shape[dim + 1 :])
    return jnp.moveaxis(value.reshape(*before, devices, -1, *after), dim, 0)


def summed_on_arrival(value, axis, dim):
    devices = lax.axis_size(axis)
    pieces = lax.all_to_all(in_blocks(value, dim, devices), axis, 0, 0, tiled=True)
    return jnp.sum(pieces.astype(jnp.float32), axis=0)


def shift_conv(padded, weights, biases, col_count):
    acc_sum = biases + jnp.zeros(padded.shape[:1] + (col_count,) + padded.shape[2:], jnp.float32)
    for offset in range(KW):
        acc_sum = acc_sum + weights[offset] * padded[:, offset : offset + col_count].astype(
            jnp.float32
        )
    return jax.nn.silu(acc_sum).astype(jnp.bfloat16)


def project(token_rows, weight):
    flat_rows = token_rows.reshape(-1, token_rows.shape[-1])
    result = jnp.dot(flat_rows, weight, preferred_element_type=jnp.float32).astype(jnp.bfloat16)
    return result.reshape(token_rows.shape[:-1] + (weight.shape[1],))


def add_totals(earlier, later_part):
    return earlier + later_part


def decayed(step_sizes, rates, values, head_count):
    rest_sum = lax.cumsum(step_sizes, axis=1, reverse=True) - step_sizes
    totals = jnp.sum(step_sizes, axis=1)
    later_sum = prefix(totals, "sp", add_totals, jnp.zeros_like(totals))
    weight = jnp.exp(rates * (rest_sum + later_sum[:, None, :])) * step_sizes
    shaped = values.astype(jnp.float32).reshape(
        values.shape[0], values.shape[1], head_count, P_SIZE
    )
    return (weight[..., None] * shaped).astype(jnp.bfloat16)


def per_device(
    x_in, x_new, w_x, w_b, w_c, w_dt, w_z, conv_w, conv_b, dt_bias, a_log, d_skip, norm_g
):
    seq_count = x_in.shape[0]
    span_len = x_in.shape[1]
    tp_size = lax.axis_size(TP)
    sp_size = lax.axis_size("sp")
    tp_rank = lax.axis_index(TP)
    sp_rank = lax.axis_index("sp")
    heads_local = H // tp_size
    groups_local = G // tp_size
    inner_cols = H * P_SIZE
    state_cols = G * N
    edge_rows = KW - 1
    decay_rates = -jnp.exp(a_log)
    bias_local = lax.dynamic_slice_in_dim(dt_bias, tp_rank * heads_local, heads_local)
    rate_local = lax.dynamic_slice_in_dim(decay_rates, tp_rank * heads_local, heads_local)
    pre_values = project(x_in, w_x)
    pre_keys = project(x_in, w_b)
    raw_steps = project(x_in, w_dt)
    pre_query = project(x_in[:, span_len - edge_rows :], w_c)
    joined = jnp.concatenate([pre_values, pre_keys], axis=2)
    before = passed_along(joined[:, span_len - edge_rows :], "sp", 1)
    conved = shift_conv(
        jnp.concatenate([before, joined], axis=1),
        conv_w[:, : inner_cols + state_cols],
        conv_b[: inner_cols + state_cols],
        span_len,
    )
    tail_rows = jnp.concatenate([joined[:, span_len - edge_rows :], pre_query], axis=2)
    last_rows = broadcast(tail_rows, "sp", sp_size - 1)
    all_tails = gather_axes(last_rows, ("tp_0", "tp_1"), (0, 1), 0)
    step_sizes = jax.nn.softplus(raw_steps.astype(jnp.float32) + dt_bias)
    scaled = decayed(step_sizes, decay_rates, conved[..., :inner_cols], H)
    key_rows = conved[..., inner_cols:].reshape(seq_count, span_len, G, N)
    term_full = jnp.einsum(
        "slgrp,slgn->sgrpn",
        scaled.reshape(seq_count, span_len, G, R, P_SIZE),
        key_rows,
        preferred_element_type=jnp.float32,
    ).reshape(seq_count, H, P_SIZE, N)
    term_rows = lax.all_to_all(
        term_full.astype(jnp.bfloat16), TP, split_axis=1, concat_axis=0, tiled=True
    ).astype(term_full.dtype)
    state_piece = summed_on_arrival(term_rows.astype(jnp.bfloat16), "sp", 0)
    state_cache = state_piece.astype(jnp.bfloat16)
    seq_local = state_piece.shape[0]
    tails_local = lax.dynamic_slice_in_dim(all_tails, sp_rank * seq_local, seq_local, 0)
    value_cols = tp_rank * heads_local * P_SIZE
    group_cols = tp_rank * groups_local * N
    new_values = jnp.dot(
        x_new,
        lax.dynamic_slice_in_dim(w_x, value_cols, heads_local * P_SIZE, 1),
        preferred_element_type=jnp.float32,
    ).astype(jnp.bfloat16)
    new_keys = jnp.dot(
        x_new,
        lax.dynamic_slice_in_dim(w_b, group_cols, groups_local * N, 1),
        preferred_element_type=jnp.float32,
    ).astype(jnp.bfloat16)
    new_query = jnp.dot(
        x_new,
        lax.dynamic_slice_in_dim(w_c, group_cols, groups_local * N, 1),
        preferred_element_type=jnp.float32,
    ).astype(jnp.bfloat16)
    new_raw = jnp.dot(
        x_new,
        lax.dynamic_slice_in_dim(w_dt, tp_rank * heads_local, heads_local, 1),
        preferred_element_type=jnp.float32,
    ).astype(jnp.bfloat16)
    gate_new = jnp.dot(x_new, w_z, preferred_element_type=jnp.float32).astype(jnp.bfloat16)

    def new_conv(newest, col_start, col_count):
        history = lax.dynamic_slice_in_dim(tails_local, col_start, col_count, 2)
        padded = jnp.concatenate([history, newest[:, None, :]], axis=1)
        return shift_conv(
            padded,
            lax.dynamic_slice_in_dim(conv_w, col_start, col_count, 1),
            lax.dynamic_slice_in_dim(conv_b, col_start, col_count, 0),
            1,
        )[:, 0]

    conv_values = new_conv(new_values, value_cols, heads_local * P_SIZE)
    value_rows = conv_values.astype(jnp.float32).reshape(seq_local, groups_local, R, P_SIZE)
    conv_keys = new_conv(new_keys, inner_cols + group_cols, groups_local * N)
    conv_keys = conv_keys.astype(jnp.float32).reshape(seq_local, groups_local, N)
    conv_query = new_conv(new_query, inner_cols + state_cols + group_cols, groups_local * N)
    conv_query = conv_query.astype(jnp.float32).reshape(seq_local, groups_local, N)
    new_steps = jax.nn.softplus(new_raw.astype(jnp.float32) + bias_local)
    decay_new = jnp.exp(rate_local * new_steps).reshape(seq_local, groups_local, R)
    held_read = jnp.einsum(
        "sgrpn,sgn->sgrp", state_piece.reshape(seq_local, groups_local, R, P_SIZE, N), conv_query
    )
    inner_prod = jnp.sum(conv_query * conv_keys, axis=-1)
    step_group = new_steps.reshape(seq_local, groups_local, R)
    skip_local = lax.dynamic_slice_in_dim(d_skip, tp_rank * heads_local, heads_local).reshape(
        groups_local, R
    )
    output = (
        decay_new[..., None] * held_read
        + (step_group * inner_prod[:, :, None])[..., None] * value_rows
        + skip_local[None, :, :, None] * value_rows
    )
    gate_rows = gate_new.astype(jnp.float32).reshape(seq_local, groups_local, R, P_SIZE)
    gated_out = output * jax.nn.silu(gate_rows)
    group_ms = jnp.mean(gated_out * gated_out, axis=(2, 3))
    read_out = (
        gated_out
        * lax.rsqrt(group_ms + eps)[:, :, None, None]
        * norm_g.reshape(groups_local, R, P_SIZE)
    )
    read_out = read_out.astype(jnp.bfloat16).reshape(seq_local, heads_local, P_SIZE)
    return (state_cache, read_out)


def solution(mesh):
    finer = Mesh(mesh.devices.reshape(mesh.shape["sp"], 4, 2), ("sp", "tp_0", "tp_1"))
    return jax.shard_map(
        per_device,
        mesh=finer,
        in_specs=(
            P(TP, "sp", None),
            P("sp", None),
            P(),
            P(),
            P(),
            P(),
            P(None, TP),
            P(),
            P(),
            P(),
            P(),
            P(),
            P(TP, None),
        ),
        out_specs=(P("sp", TP, None, None), P("sp", TP, None)),
        check_vma=False,
    )
```

profile of v0, /device:TPU:0, one launch (start us, length us, event | category | flops | bytes accessed | tf_op | source)
XLA Modules:
  0.0 158.0 jit_solution(8769843090585375116)
XLA Ops:
  0.7 3.0 %fusion.8 = f32[768,32]{0,1:T(8,128)S(1)} fusion(bf16[768,2048]{1,0:T(8,128)(2,1)} %bitcast.261, bf16[2048,32]{0,1:T(8,128)(2,1)} %param.18), kind=kOutput, calls=%fused_computation.16 | convolution fusion | flops 100712448 | bytes 3375104 | tf_op jit(solution)/shard_map/dot_general | solution.py:96
  4.5 8.0 %all-to-all-start = ((f32[16,2,32]{2,1,0:T(2,128)}), f32[16,2,32]{2,1,0:T(2,128)S(1)}, u32[]{:S(2)}, u32[]{:S(2)}) async-start(f32[16,2,32]{2,1,0:T(2,128)} %broadcast_in_dim.21), calls=%async_computation | async-start | bytes 32768 | tf_op jit(solution)/shard_map/all_to_all | solution.py:21
  12.5 7.7 %convolution_convert_fusion.1 = bf16[768,1024]{1,0:T(8,128)(2,1)} fusion(bf16[768,2048]{1,0:T(8,128)(2,1)} %bitcast.262, bf16[2048,1024]{1,0:T(8,128)(2,1)} %param.16), kind=kOutput, calls=%fused_computation.12 | convolution fusion | flops 3222011904 | bytes 8912896 | tf_op jit(solution)/shard_map/dot_general | solution.py:96
  20.2 1.9 %copy.66 = bf16[2,384,1024]{1,2,0:T(8,128)(2,1)S(1)} copy(bf16[2,384,1024]{2,1,0:T(8,128)(2,1)} %bitcast.267) | data formatting | bytes 3145728 | tf_op jit(solution)/shard_map/reshape | solution.py:97
  22.1 11.9 %convolution_convert_fusion = bf16[768,2048]{1,0:T(8,128)(2,1)} fusion(bf16[768,2048]{1,0:T(8,128)(2,1)} %bitcast.263, bf16[2048,2048]{1,0:T(8,128)(2,1)} %param.15), kind=kOutput, calls=%fused_computation.7 | convolution fusion | flops 6444023808 | bytes 14680064 | tf_op jit(solution)/shard_map/dot_general | solution.py:96
  34.0 4.6 %copy.65 = bf16[2,384,2048]{1,2,0:T(8,128)(2,1)} copy(bf16[2,384,2048]{2,1,0:T(8,128)(2,1)} %bitcast.265) | data formatting | bytes 6291456 | tf_op jit(solution)/shard_map/reshape | solution.py:97
  38.6 2.9 %fusion.4 = bf16[2,3,3072]{1,2,0:T(8,128)(2,1)} fusion(bf16[2,384,2048]{1,2,0:T(8,128)(2,1)} %copy.65, bf16[2,384,1024]{1,2,0:T(8,128)(2,1)S(1)} %copy.66), kind=kLoop, calls=%fused_computation.13 | loop fusion | flops 73728 | bytes 4755456 | tf_op jit(solution)/shard_map/concatenate | solution.py:136
  41.6 2.4 %copy.67 = bf16[2,3,3072]{2,0,1:T(2,128)(2,1)} copy(bf16[2,3,3072]{1,2,0:T(8,128)(2,1)} %fusion.4) | data formatting | bytes 73728 | tf_op jit(solution)/shard_map/slice | solution.py:137
  43.9 4.0 %collective-permute-start = (bf16[2,3,3072]{2,0,1:T(2,128)(2,1)}, bf16[2,3,3072]{2,0,1:T(2,128)(2,1)S(1)}, u32[]{:S(2)}, u32[]{:S(2)}) collective-permute-start(bf16[2,3,3072]{2,0,1:T(2,128)(2,1)} %copy.67), channel_id=1, source_target_pairs={{0,8},{8,16},{16,24},{24,32},{32,40},{40,48},{48,56},{56,64},{64,7... | collective-permute-start | bytes 110600 | tf_op jit(solution)/shard_map/ppermute | solution.py:47
  49.5 2.8 %convolution_convert_fusion.3 = bf16[6,1024]{1,0:T(8,128)(2,1)S(1)} fusion(bf16[6,2048]{1,0:T(8,128)(2,1)S(1)} %reshape.243, bf16[2048,1024]{1,0:T(8,128)(2,1)} %param.17), kind=kOutput, calls=%fused_computation.17 | convolution fusion | flops 25171968 | bytes 4231168 | tf_op jit(solution)/shard_map/dot_general | solution.py:96
  52.4 7.5 %reduce-window.6 = f32[2,32,3,128]{3,1,2,0:T(8,128)S(1)} reduce-window(f32[2,32,3,128]{3,1,2,0:T(8,128)S(1)} %bitcast.276, f32[]{:T(128)} %constant.97.clone.1), window={size=1x1x1x128 pad=0_0x0_0x0_0x0_127}, to_apply=%region_0.1 | reduce-window | flops 3121152 | bytes 196612 | tf_op jit(solution)/shard_map/reduce-window
  60.3 3.2 %pad_maximum_fusion.1 = bf16[2,3,4096]{1,2,0:T(8,128)(2,1)} fusion(bf16[2,3,1024]{1,2,0:T(8,128)(2,1)S(1)} %copy.74, bf16[2,3,3072]{1,2,0:T(8,128)(2,1)} %fusion.4), kind=kLoop, calls=%fused_computation.10 | loop fusion | flops 98304 | bytes 98304 | tf_op jit(solution)/shard_map/concatenate | solution.py:144
  66.7 1.6 %copy.68 = bf16[2,3,3072]{1,2,0:T(8,128)(2,1)} copy(bf16[2,3,3072]{2,0,1:T(2,128)(2,1)S(1)} %collective-permute-done) | data formatting | bytes 73728 | tf_op jit(solution)/shard_map/ppermute | solution.py:47
  68.3 8.2 %maximum_maximum_fusion = bf16[2,387,3072]{1,2,0:T(8,128)(2,1)S(1)} fusion(bf16[2,384,1024]{1,2,0:T(8,128)(2,1)S(1)} %copy.66, bf16[2,384,2048]{1,2,0:T(8,128)(2,1)} %copy.65, bf16[2,3,3072]{1,2,0:T(8,128)(2,1)} %copy.68), kind=kLoop, calls=%fused_computation.1 | loop fusion | flops 14266368 | bytes 9510912 | tf_op jit(solution)/shard_map/concatenate | solution.py:139
  76.5 10.8 %multiply_convert_fusion = bf16[2,384,3072]{1,2,0:T(8,128)(2,1)S(1)} fusion(bf16[2,384,1024]{1,2,0:T(8,128)(2,1)S(1)} %copy.66, bf16[2,384,2048]{1,2,0:T(8,128)(2,1)S(1)} %copy-done.1, bf16[2,387,3072]{1,2,0:T(8,128)(2,1)S(1)} %maximum_maximum_fusion, f32[3072]{0:T(1024)S(1)} %bitcast.279, f32[3072]{0:T(1024)S(1)} %bitcast.280, f32[3072]{0:T(1024)S(1)} %bitcast.281, ...), kind=kLoop, calls=%fused_computation | loop fusion | flops 47185920 | bytes 23654400 | tf_op jit(solution)/shard_map/convert_element_type | solution.py:91
  90.0 4.6 %all-to-all-start.1 = ((bf16[2,32,64,128]{3,2,0,1:T(8,128)(2,1)}), bf16[2,32,64,128]{3,2,0,1:T(8,128)(2,1)}, u32[]{:S(2)}, u32[]{:S(2)}) async-start(bf16[2,32,64,128]{3,2,0,1:T(8,128)(2,1)} %copy.70), calls=%async_computation.1 | async-start | bytes 2097152 | tf_op jit(solution)/shard_map/all_to_all | solution.py:156
  95.6 25.1 %all-gather = bf16[32,3,4096]{2,1,0:T(4,128)(2,1)S(1)} all-gather(bf16[2,3,4096]{2,1,0:T(4,128)(2,1)S(1)} %copy.75), channel_id=2, replica_groups=mesh['sp'=16,'tp_0'=4,'tp_1'=2] {'sp'}, dimensions={0}, use_global_device_ids=true | all-gather | bytes 835584 | tf_op jit(solution)/shard_map/all_gather | solution.py:51
  120.7 12.7 %all-gather.1 = bf16[8,3,4096]{2,1,0:T(4,128)(2,1)S(1)} all-gather(bf16[2,3,4096]{2,1,0:T(4,128)(2,1)S(1)} %slice.201), channel_id=3, replica_groups=mesh['sp'=16,'tp_0'=4,'tp_1'=2] {'tp_0'}, dimensions={0}, use_global_device_ids=true | all-gather | bytes 245760 | tf_op jit(solution)/shard_map/all_gather | solution.py:63
  135.1 2.3 %copy.72 = bf16[8,2,4,64,128]{4,3,2,1,0:T(8,128)(2,1)} copy(bf16[8,2,4,64,128]{4,3,1,2,0:T(8,128)(2,1)} %bitcast.17) | data formatting | bytes 2097152 | tf_op jit(solution)/shard_map/all_to_all | solution.py:156
  137.5 4.9 %all-to-all-start.2 = ((bf16[16,1,4,64,128]{4,3,2,1,0:T(8,128)(2,1)}), bf16[16,1,4,64,128]{4,3,2,1,0:T(8,128)(2,1)S(1)}, u32[]{:S(2)}, u32[]{:S(2)}) async-start(bf16[16,1,4,64,128]{4,3,2,1,0:T(8,128)(2,1)} %bitcast.19), calls=%async_computation.2 | async-start | bytes 2097152 | tf_op jit(solution)/shard_map/all_to_all | solution.py:81
  142.4 2.1 %all_gather.15 = bf16[8,2,3,4096]{3,1,2,0:T(2,128)(2,1)S(1)} all-gather(bf16[4,2,3,4096]{3,1,2,0:T(2,128)(2,1)S(1)} %copy.76), channel_id=1, replica_groups=mesh['sp'=16,'tp_0'=4,'tp_1'=2] {'tp_1'}, dimensions={0}, use_global_device_ids=true | all-gather | bytes 589824 | tf_op jit(solution)/shard_map/all_gather | solution.py:63
  146.5 1.9 %multiply_reduce_fusion.1 = f32[]{:T(128)} fusion(bf16[1,2048]{1,0:T(2,128)(2,1)S(1)} %copy-done.4, bf16[2048,1024]{1,0:T(8,128)(2,1)} %param.16, s32[]{:T(128)S(6)} %select_n.62, f32[4,128]{1,0:T(4,128)S(1)} %get-tuple-element.9, bf16[1,3,128]{2,1,0:T(4,128)(2,1)S(1)} %get-tuple-element.5, f32[4096]{0:T(1024)S(1)} %copy-done.6, s32[]{:T(128)S(6)} %select_n.63, ...), kind=kOutput, calls=%fused_computation.113 | convolution fusion | flops 527103 | bytes 531980 | tf_op jit(solution)/shard_map/dot_general | solution.py:170
  148.3 1.5 multiply_exponential_fusion
  149.9 5.9 %all-to-all-done.2 = bf16[16,1,4,64,128]{4,3,2,1,0:T(8,128)(2,1)S(1)} async-done(((bf16[16,1,4,64,128]{4,3,2,1,0:T(8,128)(2,1)}), bf16[16,1,4,64,128]{4,3,2,1,0:T(8,128)(2,1)S(1)}, u32[]{:S(2)}, u32[]{:S(2)}) %all-to-all-start.2) | async-done | bytes 1048608 | tf_op jit(solution)/shard_map/all_to_all | solution.py:81
  (84 shorter events, 14.8 us)
Async XLA Ops:
  0.6 62.9 %copy-start = (bf16[2048,256]{1,0:T(8,128)(2,1)S(1)}, bf16[2048,256]{1,0:T(8,128)(2,1)}, u32[]{:S(2)}) copy-start(bf16[2048,256]{1,0:T(8,128)(2,1)} %param.19) | copy-start | bytes 3145732
  0.6 3.0 %copy-start.10 = (f32[32]{0:T(128)S(1)}, f32[32]{0:T(128)}, u32[]{:S(2)}) copy-start(f32[32]{0:T(128)} %param.22) | copy-start | bytes 388
  4.5 61.1 %all-to-all-start = ((f32[16,2,32]{2,1,0:T(2,128)}), f32[16,2,32]{2,1,0:T(2,128)S(1)}, u32[]{:S(2)}, u32[]{:S(2)}) async-start(f32[16,2,32]{2,1,0:T(2,128)} %broadcast_in_dim.21), calls=%async_computation | async-start | bytes 32768 | tf_op jit(solution)/shard_map/all_to_all | solution.py:21
  38.6 10.2 %copy-start.14 = (f32[32]{0:T(128)S(1)}, f32[32]{0:T(128)}, u32[]{:S(2)}) copy-start(f32[32]{0:T(128)} %param.23) | copy-start | bytes 388
  41.6 10.8 %copy-start.5 = (f32[4,4096]{1,0:T(4,128)S(1)}, f32[4,4096]{1,0:T(4,128)}, u32[]{:S(2)}) copy-start(f32[4,4096]{1,0:T(4,128)} %param.20) | copy-start | bytes 196612
  43.9 22.7 %collective-permute-start = (bf16[2,3,3072]{2,0,1:T(2,128)(2,1)}, bf16[2,3,3072]{2,0,1:T(2,128)(2,1)S(1)}, u32[]{:S(2)}, u32[]{:S(2)}) collective-permute-start(bf16[2,3,3072]{2,0,1:T(2,128)(2,1)} %copy.67), channel_id=1, source_target_pairs={{0,8},{8,16},{16,24},{24,32},{32,40},{40,48},{48,56},{56,64},{64,7... | collective-permute-start | bytes 110600 | tf_op jit(solution)/shard_map/ppermute | solution.py:47
  49.5 14.1 %copy-start.4 = (bf16[1,2048]{1,0:T(2,128)(2,1)S(1)}, bf16[1,2048]{1,0:T(2,128)(2,1)}, u32[]{:S(2)}) copy-start(bf16[1,2048]{1,0:T(2,128)(2,1)} %param.14) | copy-start | bytes 12292
  52.3 12.0 %copy-start.6 = (f32[4096]{0:T(1024)S(1)}, f32[4096]{0:T(1024)}, u32[]{:S(2)}) copy-start(f32[4096]{0:T(1024)} %param.21) | copy-start | bytes 49156
  68.3 8.2 %copy-start.1 = (bf16[2,384,2048]{1,2,0:T(8,128)(2,1)S(1)}, bf16[2,384,2048]{1,2,0:T(8,128)(2,1)}, u32[]{:S(2)}) copy-start(bf16[2,384,2048]{1,2,0:T(8,128)(2,1)} %copy.65) | copy-start | bytes 9437188
  68.3 8.2 %slice-start = ((f32[4096]{0:T(1024)}), f32[3072]{0:T(1024)S(1)}, s32[]{:S(2)}) async-start(f32[4096]{0:T(1024)} %param.21), calls=%async_computation.3 | async-start | bytes 24576 | tf_op jit(solution)/shard_map/slice | solution.py:141
  87.8 6.7 %copy-start.7 = (f32[1,256]{1,0:T(1,128)S(1)}, f32[1,256]{1,0:T(1,128)}, u32[]{:S(2)}) copy-start(f32[1,256]{1,0:T(1,128)} %fusion.32) | copy-start | bytes 3076
  87.9 6.8 %copy-start.2 = (bf16[2,3,4096]{1,2,0:T(8,128)(2,1)S(1)}, bf16[2,3,4096]{1,2,0:T(8,128)(2,1)}, u32[]{:S(2)}) copy-start(bf16[2,3,4096]{1,2,0:T(8,128)(2,1)} %pad_maximum_fusion.1) | copy-start | bytes 147460
  90.0 45.1 %copy-start.8 = (f32[1,256]{1,0:T(1,128)S(1)}, f32[1,256]{1,0:T(1,128)}, u32[]{:S(2)}) copy-start(f32[1,256]{1,0:T(1,128)} %dynamic-slice.6) | copy-start | bytes 3076
  90.0 45.2 %all-to-all-start.1 = ((bf16[2,32,64,128]{3,2,0,1:T(8,128)(2,1)}), bf16[2,32,64,128]{3,2,0,1:T(8,128)(2,1)}, u32[]{:S(2)}, u32[]{:S(2)}) async-start(bf16[2,32,64,128]{3,2,0,1:T(8,128)(2,1)} %copy.70), calls=%async_computation.1 | async-start | bytes 2097152 | tf_op jit(solution)/shard_map/all_to_all | solution.py:156
  95.6 49.3 %copy-start.9 = (f32[256]{0:T(256)S(1)}, f32[256]{0:T(256)}, u32[]{:S(2)}) copy-start(f32[256]{0:T(256)} %dynamic_slice.68) | copy-start | bytes 3076
  95.6 49.5 %copy-start.15 = (f32[32]{0:T(128)S(1)}, f32[32]{0:T(128)}, u32[]{:S(2)}) copy-start(f32[32]{0:T(128)} %param.24) | copy-start | bytes 388
  133.4 14.9 %copy-start.11 = (f32[32]{0:T(128)S(1)}, f32[32]{0:T(128)}, u32[]{:S(2)}) copy-start(f32[32]{0:T(128)} %param.22) | copy-start | bytes 388
  133.4 14.9 %copy-start.13 = (f32[32]{0:T(128)S(1)}, f32[32]{0:T(128)}, u32[]{:S(2)}) copy-start(f32[32]{0:T(128)} %exponential_negate_fusion) | copy-start | bytes 388
  135.1 22.3 %copy-start.12 = (f32[4,64]{1,0:T(4,128)S(1)}, f32[4,64]{1,0:T(4,128)}, u32[]{:S(2)}) copy-start(f32[4,64]{1,0:T(4,128)} %param.25) | copy-start | bytes 3076
  137.5 18.3 %all-to-all-start.2 = ((bf16[16,1,4,64,128]{4,3,2,1,0:T(8,128)(2,1)}), bf16[16,1,4,64,128]{4,3,2,1,0:T(8,128)(2,1)S(1)}, u32[]{:S(2)}, u32[]{:S(2)}) async-start(bf16[16,1,4,64,128]{4,3,2,1,0:T(8,128)(2,1)} %bitcast.19), calls=%async_computation.2 | async-start | bytes 2097152 | tf_op jit(solution)/shard_map/all_to_all | solution.py:81
  155.9 2.1 %copy-start.3 = (bf16[4,64,128]{2,1,0:T(8,128)(2,1)}, bf16[4,64,128]{2,1,0:T(8,128)(2,1)S(1)}, u32[]{:S(2)}) copy-start(bf16[4,64,128]{2,1,0:T(8,128)(2,1)S(1)} %convert_reduce_fusion) | copy-start | bytes 196612
where the time goes:
time: 159 us; the launch traced here: 158 us
  blocking collectives  39.8 us (25%)
  other arithmetic  35.9 us (23%)
  matrix products  33.5 us (21%)
  starting transfers between devices  21.5 us (14%)
  local copies, waits for them, and re-layouts  19.6 us (12%)
  waiting for transfers between devices  5.88 us (4%)
  between operations  1.71 us (1%)
    dot_general x4, matrix products, project(): jnp.dot(flat_rows, weight, preferred_element_type=jnp.float32)  25.4 us
    all_gather x1, blocking collectives, broadcast(): lax.all_gather(value, axis)  25.1 us
    all_gather x2, blocking collectives, all_blocks(): pieces = lax.all_gather(pieces, axes[k], axis=0, tiled=True)  14.8 us
    convert_element_type x1, other arithmetic, shift_conv(): return jax.nn.silu(acc_sum).astype(jnp.bfloat16)  10.8 us
    concatenate x1, other arithmetic, per_device(): jnp.concatenate([before, joined], axis=1)  8.2 us
    all_to_all x1, starting transfers between devices, copy_for_each(): return lax.all_to_all(copies, axis, split_axis=0, concat_axis=0, tiled=True)  7.99 us
    another operation x2, other arithmetic  7.5 us
    reshape x4, local copies, waits for them, and re-layouts, project(): return result.reshape(token_rows.shape[:-1] + (weight.shape[1],))  6.86 us
  transfers between devices with their start and end apart: 4, of which 1 were waited for; matrix products, arithmetic and copies ran while one was open for 37% of the time, Pallas kernels for 0%

commit v1 on v0

v1 whole, which is shorter than its diff:
```python
import jax
import jax.numpy as jnp
from jax import lax
from jax.experimental import pallas as pl
from jax.experimental.pallas import tpu as pltpu
from jax.sharding import PartitionSpec as P

H = 32
P_SIZE = 64
G = 8
N = 128
KW = 4
R = 4
D = 2048
T = 384
eps = 1e-05
MESH = pl.DeviceIdType.MESH
BF = jnp.bfloat16
F32 = jnp.float32
OFFS = (2, 1, 3, 0)
SP = 16


def dot(a, b):
    return jnp.dot(a, b, preferred_element_type=F32)


def dot_exact(a, b):
    return jnp.dot(a, b, preferred_element_type=F32, precision=lax.Precision.HIGHEST)


def softplus(v):
    return jnp.maximum(v, 0.0) + jnp.log1p(jnp.exp(-jnp.abs(v)))


def kernel(
    x_hbm, xnew_ref, wx_hbm, wb_hbm, wc_hbm, wdt_hbm, wz_hbm,
    cw_ref, cb_ref, dtb_ref, alog_ref, dskip_ref, ng_ref,
    st_out, ro_out,
    x_ref, wx_ref, wb_ref, wc_ref, wdt_ref, wz_ref,
    pre_refs, key_refs, sc_refs, wg_ref, fac_ref,
    edge_tx, halo_rx, tail_rx, tot_tx, tot_rx,
    tx1, rx1, tx2, rx2,
    in_sems, w_sems,
    halo_s, halo_r, tail_s, tail_r, tot_s, tot_r, s1_s, s1_r, s2_s, s2_r,
):
    i = lax.axis_index("sp")
    j = lax.axis_index("tp")
    zp, xp = i // 4, i % 4
    yp, cp = j // 2, j % 2
    other = 1 - cp

    def pair(t):
        return (yp + OFFS[t]) % 4

    x_copies = [
        pltpu.make_async_copy(x_hbm.at[s], x_ref.at[pl.ds(T * s, T), :], in_sems.at[s])
        for s in range(2)
    ]
    wdt_copy = pltpu.make_async_copy(wdt_hbm, wdt_ref, in_sems.at[2])
    wz_copy = pltpu.make_async_copy(wz_hbm, wz_ref, in_sems.at[3])
    wc_copy = pltpu.make_async_copy(
        wc_hbm.at[:, pl.ds(pl.multiple_of(j * N, N), N)], wc_ref, in_sems.at[4]
    )

    def w_copy(t):
        q = pair(t)
        kcols = pl.ds(pl.multiple_of(q * 256, 256), 256)
        vcols = pl.ds(pl.multiple_of(q * 512, 512), 512)
        return [
            pltpu.make_async_copy(wb_hbm.at[:, kcols], wb_ref.at[:, kcols], w_sems.at[t, 0]),
            pltpu.make_async_copy(wx_hbm.at[:, vcols], wx_ref.at[:, vcols], w_sems.at[t, 1]),
        ]

    wdt_copy.start()
    x_copies[0].start()
    x_copies[1].start()
    for t in range(4):
        for c in w_copy(t):
            c.start()
    wz_copy.start()
    wc_copy.start()

    bar = pltpu.get_barrier_semaphore()

    def sig(sp, tp):
        pl.semaphore_signal(bar, inc=1, device_id=(sp, tp), device_id_type=MESH)

    for d in range(1, SP):
        sig((i + d) % SP, j)

    @pl.when(cp != xp // 2)
    def _():
        for d in range(4):
            sig(zp * 4 + d, 2 * yp + other)

    for d in range(4):
        @pl.when((d != zp) | (yp != zp))
        def _():
            sig(d * 4 + xp, 2 * zp + cp)

    tail_tp = i // 2

    @pl.when((i != SP - 1) | (j != tail_tp))
    def _():
        sig(SP - 1, tail_tp)

    wdt_copy.wait()
    x_copies[0].wait()
    x_copies[1].wait()
    lo = x_ref[T - 16:T, :].astype(F32)[13:16]
    hi = x_ref[2 * T - 16:2 * T, :].astype(F32)[13:16]
    edge_tx[...] = jnp.concatenate([lo, hi, jnp.zeros((2, D), F32)], axis=0).astype(BF)
    raw = dot(x_ref[0:2 * T, :], wdt_ref[...])
    steps = softplus(raw + dtb_ref[...])
    tot_tx[...] = jnp.zeros_like(tot_tx)
    rates = -jnp.exp(alog_ref[...])
    upper = (
        lax.broadcasted_iota(jnp.int32, (T, T), 1) > lax.broadcasted_iota(jnp.int32, (T, T), 0)
    ).astype(F32).astype(BF)
    for s in range(2):
        own = steps[T * s:T * (s + 1)]
        tot_tx[s:s + 1, 0:H] = jnp.sum(own, axis=0, keepdims=True)
        high = own.astype(BF)
        low = (own - high.astype(F32)).astype(BF)
        rest = dot(upper, high) + dot(upper, low)
        weight = jnp.exp(rates * rest) * own
        for g in range(G):
            wg_ref[g, T * s:T * (s + 1), 0:R] = weight[:, R * g:R * (g + 1)]

    def w_slices(t):
        q = pair(t)
        return [
            wb_ref[:, pl.ds(pl.multiple_of(q * 256, 256), 256)],
            wx_ref[:, pl.ds(pl.multiple_of(q * 512, 256), 256)],
            wx_ref[:, pl.ds(pl.multiple_of(q * 512 + 256, 256), 256)],
        ]

    def put_halo(pre, rows):
        for c in range(2):
            pre[c, 5:8, :] = rows[0:3, 128 * c:128 * (c + 1)]
            pre[c, T + 13:T + 16, :] = rows[3:6, 128 * c:128 * (c + 1)]

    def proj(pre, w, s, halo):
        rows = T + (16 if halo and s == 1 else 0)
        res = dot(x_ref[T * s:T * s + rows, :], w)
        for c in range(2):
            pre[c, (T + 8) * s + 8:(T + 8) * (s + 1), :] = res[0:T, 128 * c:128 * (c + 1)]
        if halo and s == 1:
            put_halo(pre, res[T:T + 8])

    for c in w_copy(0):
        c.wait()
    for u, w in enumerate(w_slices(0)):
        for s in range(2):
            proj(pre_refs[u], w, s, False)

    s1_self = (cp == xp // 2)
    arrivals = 15 + 2 + 4 - jnp.where(zp == yp, 1, 0)
    arrivals = arrivals + jnp.where(i == SP - 1, 16 - jnp.where(j == 7, 1, 0), 0)
    pl.semaphore_wait(bar, arrivals)

    halo_copy = pltpu.make_async_remote_copy(
        edge_tx, halo_rx, halo_s, halo_r, device_id=((i + 1) % SP, j), device_id_type=MESH
    )
    halo_copy.start()

    def tot_copy(d):
        return pltpu.make_async_remote_copy(
            tot_tx, tot_rx.at[i], tot_s.at[d], tot_r.at[i],
            device_id=((i + d) % SP, j), device_id_type=MESH,
        )

    for d in range(1, SP):
        tot_copy(d).start()

    def tail_copy(n):
        return pltpu.make_async_remote_copy(
            edge_tx, tail_rx, tail_s.at[n], tail_r,
            device_id=(2 * j + n % 2, n // 2), device_id_type=MESH,
        )

    def tail_self(n):
        return (j == 7) & (2 * j + n % 2 == i) & (n // 2 == j)

    @pl.when(i == SP - 1)
    def _():
        for n in range(16):
            @pl.when(jnp.logical_not(tail_self(n)))
            def _():
                tail_copy(n).start()

    @pl.when((i == SP - 1) & (j == 7))
    def _():
        tail_rx[...] = edge_tx[...]

    halo_copy.wait_recv()
    keep = jnp.where(i > 0, 1.0, 0.0).astype(F32)
    halo = jnp.where(i > 0, halo_rx[...].astype(F32), 0.0)
    x_ref[2 * T:2 * T + 16, :] = jnp.concatenate([halo, jnp.zeros((8, D), F32)], axis=0).astype(BF)
    for u, w in enumerate(w_slices(0)):
        put_halo(pre_refs[u], dot(x_ref[2 * T:2 * T + 16, :], w)[0:8])

    for d in range(1, SP):
        src = (i + SP - d) % SP
        pltpu.make_async_remote_copy(
            tot_tx, tot_rx.at[src], tot_s.at[d], tot_r.at[src],
            device_id=((i + d) % SP, j), device_id_type=MESH,
        ).wait_recv()
    later = jnp.zeros((2, 128), F32)
    for d in range(SP):
        later = later + jnp.where(i < d, tot_rx[d], 0.0)
    factor = jnp.exp(rates * later[:, 0:H])
    spread = (
        lax.broadcasted_iota(jnp.int32, (H, H * P_SIZE), 1) // P_SIZE
        == lax.broadcasted_iota(jnp.int32, (H, H * P_SIZE), 0)
    ).astype(F32)
    wide = dot_exact(jnp.concatenate([factor, jnp.zeros((6, H), F32)], axis=0), spread)
    for g in range(G):
        fac_ref[g] = wide[:, 256 * g:256 * (g + 1)]

    lane = lax.broadcasted_iota(jnp.int32, (128, 128), 1)

    def conv(pre, s, c, r, off):
        cols = pl.ds(pl.multiple_of(off + 128 * c, 128), 128)
        taps = cw_ref[:, cols] * 0.5
        acc = cb_ref[:, cols] * 0.5 + taps[3:4] * pre[c, pl.ds((T + 8) * s + 8 + r, 128), :]
        for k in range(3):
            acc = acc + taps[k:k + 1] * pre[c, pl.ds((T + 8) * s + 5 + k + r, 128), :]
        return acc + acc * jnp.tanh(acc)

    def post_keys(t, s):
        q = pair(t)
        for c in range(2):
            for r in range(0, T, 128):
                out = conv(pre_refs[3 * (t % 2)], s, c, r, H * P_SIZE + q * 256)
                key_refs[t % 2][T * s + r:T * s + r + 128, 128 * c:128 * (c + 1)] = out.astype(BF)

    def post_values(t, b, s):
        g = 2 * pair(t) + b
        for c in range(2):
            for r in range(0, T, 128):
                out = conv(pre_refs[3 * (t % 2) + 1 + b], s, c, r, g * 256)
                w = wg_ref[g, pl.ds(T * s + r, 128), 0:R]
                w = jnp.where(lane < P_SIZE, w[:, 2 * c:2 * c + 1], w[:, 2 * c + 1:2 * c + 2])
                sc_refs[b][T * s + r:T * s + r + 128, 128 * c:128 * (c + 1)] = (out * w).astype(BF)

    def s1_copy(t, a, b):
        n = 4 * t + 2 * a + b
        return pltpu.make_async_remote_copy(
            tx1.at[n], rx1.at[t, xp], s1_s.at[n], s1_r.at[t, xp],
            device_id=(zp * 4 + 2 * cp + a, 2 * yp + b), device_id_type=MESH,
        )

    def s1_own(a, b):
        return (xp == 2 * cp + a) & (cp == b)

    def contract(t, a, b):
        g = 2 * pair(t) + b
        keys = key_refs[t % 2][T * a:T * (a + 1), 128 * b:128 * (b + 1)]
        term = lax.dot_general(
            keys, sc_refs[b][T * a:T * (a + 1), :], (((0,), (0,)), ((), ())),
            preferred_element_type=F32,
        )
        term = term * fac_ref[g, a:a + 1, :]
        tx1[4 * t + 2 * a + b] = term.astype(BF)

    def send1(t, a, b):
        @pl.when(jnp.logical_not(s1_own(a, b)))
        def _():
            s1_copy(t, a, b).start()

        @pl.when(s1_own(a, b))
        def _():
            rx1[t, xp] = tx1[4 * t + 2 * a + b]

    def s2_copy(t):
        return pltpu.make_async_remote_copy(
            tx2.at[t], rx2.at[zp], s2_s.at[t], s2_r.at[zp],
            device_id=(yp * 4 + xp, 2 * pair(t) + cp), device_id_type=MESH,
        )

    def s2_self(t):
        return (yp == zp) if OFFS[t] == 0 else None

    def stage2(t):
        for d in range(4):
            @pl.when(jnp.logical_not((d == xp) & s1_self))
            def _():
                pltpu.make_async_remote_copy(
                    tx1.at[0], rx1.at[t, d], s1_s.at[0], s1_r.at[t, d],
                    device_id=(i, j), device_id_type=MESH,
                ).wait_recv()
        acc = rx1[t, 0].astype(F32)
        for d in range(1, 4):
            acc = acc + rx1[t, d].astype(F32)
        tx2[t] = acc.astype(BF)
        if OFFS[t] == 0:
            @pl.when(yp != zp)
            def _():
                s2_copy(t).start()

            @pl.when(yp == zp)
            def _():
                rx2[zp] = tx2[t]
        else:
            s2_copy(t).start()

    for t in range(4):
        nxt = t + 1
        if nxt < 4:
            for c in w_copy(nxt):
                c.wait()
            ws = w_slices(nxt)
        for s in range(2):
            if nxt < 4:
                proj(pre_refs[3 * (nxt % 2)], ws[0], s, True)
            post_keys(t, s)
        for b in range(2):
            for s in range(2):
                if nxt < 4:
                    proj(pre_refs[3 * (nxt % 2) + 1 + b], ws[1 + b], s, True)
                post_values(t, b, s)
                contract(t, s, b)
        for b in range(2):
            for a in range(2):
                send1(t, a, b)
        if t > 0:
            stage2(t - 1)

    wz_copy.wait()
    wc_copy.wait()

    @pl.when(jnp.logical_not((i == SP - 1) & (j == 7)))
    def _():
        tail_copy(0).wait_recv()

    ext = jnp.concatenate(
        [tail_rx[...].astype(F32), jnp.broadcast_to(xnew_ref[...].astype(F32), (8, D))], axis=0
    ).astype(BF)
    a_own = i % 2

    def fresh(w, off, width):
        res = dot(ext, w)
        cols = pl.ds(pl.multiple_of(off, 128), width)
        taps = cw_ref[:, cols] * 0.5
        acc = cb_ref[:, cols] * 0.5 + taps[3:4] * res[8:9]
        for k in range(3):
            acc = acc + taps[k:k + 1] * jnp.where(a_own == 0, res[k:k + 1], res[3 + k:4 + k])
        return acc + acc * jnp.tanh(acc)

    values = fresh(wx_ref[:, pl.ds(pl.multiple_of(j * 256, 256), 256)], j * 256, 256)
    keys = fresh(wb_ref[:, pl.ds(pl.multiple_of(j * N, N), N)], H * P_SIZE + j * N, N)
    query = fresh(wc_ref[...], H * P_SIZE + G * N + j * N, N)
    gate = dot(ext, wz_ref[...])[8:9]
    new_raw = dot(ext, wdt_ref[...])[8:9]
    new_steps = softplus(new_raw + dtb_ref[...])
    row = lax.broadcasted_iota(jnp.int32, (8, H), 0)
    packed = jnp.where(
        row == 0, new_steps, jnp.where(row == 1, jnp.exp(rates * new_steps), dskip_ref[...])
    )
    own_spread = (
        lax.broadcasted_iota(jnp.int32, (H, 256), 1) // P_SIZE + R * j
        == lax.broadcasted_iota(jnp.int32, (H, 256), 0)
    ).astype(F32)
    per_lane = dot_exact(packed, own_spread)
    step_row, decay_row, skip_row = per_lane[0:1], per_lane[1:2], per_lane[2:3]
    inner = jnp.sum(query * keys, axis=1, keepdims=True)
    direct = (step_row * inner + skip_row) * values
    gate = gate * jax.nn.sigmoid(gate)

    stage2(3)

    for d in range(4):
        @pl.when(jnp.logical_not((d == zp) & (yp == zp)))
        def _():
            pltpu.make_async_remote_copy(
                tx2.at[0], rx2.at[d], s2_s.at[0], s2_r.at[d],
                device_id=(i, j), device_id_type=MESH,
            ).wait_recv()
    state = rx2[0].astype(F32)
    for d in range(1, 4):
        state = state + rx2[d].astype(F32)
    st_out[0] = state.T.astype(BF).reshape(R, P_SIZE, N)
    held = dot_exact(jnp.broadcast_to(query, (8, N)), state)[0:1]
    gated = (decay_row * held + direct) * gate
    ms = jnp.sum(gated * gated, axis=1, keepdims=True) * (1.0 / 256)
    normed = gated * lax.rsqrt(ms + eps)
    head = lax.broadcasted_iota(jnp.int32, (R, 256), 0)
    chan = lax.broadcasted_iota(jnp.int32, (R, 256), 1) // P_SIZE
    split = jnp.where(head == chan, normed, 0.0)
    split = split[:, 0:128] + split[:, 128:256]
    split = split[:, 0:P_SIZE] + split[:, P_SIZE:128]
    ro_out[0] = (split * ng_ref[...]).astype(BF)

    halo_copy.wait_send()
    for d in range(1, SP):
        tot_copy(d).wait_send()

    @pl.when(i == SP - 1)
    def _():
        for n in range(16):
            @pl.when(jnp.logical_not(tail_self(n)))
            def _():
                tail_copy(n).wait_send()

    for t in range(4):
        for a in range(2):
            for b in range(2):
                @pl.when(jnp.logical_not(s1_own(a, b)))
                def _():
                    s1_copy(t, a, b).wait_send()
        if OFFS[t] == 0:
            @pl.when(yp != zp)
            def _():
                s2_copy(t).wait_send()
        else:
            s2_copy(t).wait_send()


def per_device(
    x_in, x_new, w_x, w_b, w_c, w_dt, w_z, conv_w, conv_b, dt_bias, a_log, d_skip, norm_g
):
    hbm = pl.BlockSpec(memory_space=pl.ANY)
    vmem = pl.BlockSpec(memory_space=pltpu.VMEM)
    dma = pltpu.SemaphoreType.DMA
    return pl.pallas_call(
        kernel,
        out_shape=(
            jax.ShapeDtypeStruct((1, R, P_SIZE, N), BF),
            jax.ShapeDtypeStruct((1, R, P_SIZE), BF),
        ),
        in_specs=[hbm, vmem, hbm, hbm, hbm, hbm, hbm] + [vmem] * 6,
        out_specs=(vmem, vmem),
        scratch_shapes=[
            pltpu.VMEM((2 * T + 16, D), BF),
            pltpu.VMEM((D, H * P_SIZE), BF),
            pltpu.VMEM((D, G * N), BF),
            pltpu.VMEM((D, N), BF),
            pltpu.VMEM((D, H), BF),
            pltpu.VMEM((D, 256), BF),
            [pltpu.VMEM((2, 2 * (T + 8), 128), F32) for _ in range(6)],
            [pltpu.VMEM((2 * T, 256), BF) for _ in range(2)],
            [pltpu.VMEM((2 * T, 256), BF) for _ in range(2)],
            pltpu.VMEM((G, 2 * T, 128), F32),
            pltpu.VMEM((G, 8, 256), F32),
            pltpu.VMEM((8, D), BF),
            pltpu.VMEM((8, D), BF),
            pltpu.VMEM((8, D), BF),
            pltpu.VMEM((2, 128), F32),
            pltpu.VMEM((SP, 2, 128), F32),
            pltpu.VMEM((16, N, 256), BF),
            pltpu.VMEM((4, 4, N, 256), BF),
            pltpu.VMEM((4, N, 256), BF),
            pltpu.VMEM((4, N, 256), BF),
            dma((5,)),
            dma((4, 2)),
            dma,
            dma,
            dma((16,)),
            dma,
            dma((SP,)),
            dma((SP,)),
            dma((16,)),
            dma((4, 4)),
            dma((4,)),
            dma((4,)),
        ],
        compiler_params=pltpu.CompilerParams(
            collective_id=0, has_side_effects=True, vmem_limit_bytes=60 * 1024 * 1024
        ),
    )(
        x_in, x_new, w_x, w_b, w_c, w_dt, w_z, conv_w,
        conv_b.reshape(1, -1), dt_bias.reshape(1, -1), a_log.reshape(1, -1),
        d_skip.reshape(1, -1), norm_g,
    )


def solution(mesh):
    return jax.shard_map(
        per_device,
        mesh=mesh,
        in_specs=(
            P("tp", "sp", None),
            P("sp", None),
            P(),
            P(),
            P(),
            P(),
            P(None, "tp"),
            P(),
            P(),
            P(),
            P(),
            P(),
            P("tp", None),
        ),
        out_specs=(P("sp", "tp", None, None), P("sp", "tp", None)),
        check_vma=False,
    )
```

time: 159 us -> 50.7 us (0.32)
  the two profiles are of different devices: /device:TPU:0 before, /device:TPU:1 now
where the time goes in v1:
time: 50.7 us; the launch traced here: 50.5 us
  Pallas kernels  45.2 us (89%)
  local copies, waits for them, and re-layouts  4.6 us (9%)
  between operations  0.64 us (1%)
    pallas_call x1, Pallas kernels, per_device(): pl.pallas_call(kernel, out_shape=(jax.ShapeDtypeStruct((1, R, P_SIZE, N),...  45.2 us
    unnamed x3, local copies, waits for them, and re-layouts  4.6 us

profile of v1, /device:TPU:1, one launch (start us, length us, event | category | flops | bytes accessed | tf_op | source)
XLA Modules:
  0.0 50.5 jit_solution(1189660558537762113)
XLA Ops:
  0.6 1.9 %copy.15.wdt_hbm = bf16[2048,32]{1,0:T(8,128)(2,1)} copy(bf16[2048,32]{0,1:T(8,128)(2,1)} %param.18) | data formatting | bytes 262144 | tf_op args[5]
  2.5 45.2 %shard_map.140 = (bf16[1,4,64,128]{3,2,1,0:T(8,128)(2,1)}, bf16[1,4,64]{2,1,0:T(4,128)(2,1)}) custom-call(bf16[2,384,2048]{2,1,0:T(8,128)(2,1)} %x_hbm.1, bf16[1,2048]{1,0:T(2,128)(2,1)} %xnew_ref.1, bf16[2048,2048]{1,0:T(8,128)(2,1)} %wx_hbm.1, bf16[2048,1024]{1,0:T(8,128)(2,1)} %wb_hbm.1, bf16[2048,1024]{1,0:T(8,128)(2,1)} %wc_hbm.1, ...), custom_call_target="tpu_custom_call" | custom-call | tf_op jit(solution)/shard_map/pallas_call | solution.py:427
  47.8 1.5 %copy.18 = bf16[1,4,64,128]{3,2,1,0:T(8,128)(2,1)} copy(bf16[1,4,64,128]{3,2,1,0:T(8,128)(2,1)} %get-tuple-element.4) | data formatting | bytes 131072
  49.3 1.2 %copy.19 = bf16[1,4,64]{2,1,0:T(4,128)(2,1)} copy(bf16[1,4,64]{2,1,0:T(4,128)(2,1)} %get-tuple-element.5) | data formatting | bytes 1024

commit v2 on v1

v2 whole, which is shorter than its diff:
```python
import jax
import jax.numpy as jnp
from jax import lax
from jax.experimental import pallas as pl
from jax.experimental.pallas import tpu as pltpu
from jax.sharding import PartitionSpec as P

H = 32
P_SIZE = 64
G = 8
N = 128
KW = 4
R = 4
D = 2048
T = 384
eps = 1e-05
MESH = pl.DeviceIdType.MESH
BF = jnp.bfloat16
F32 = jnp.float32
OFFS = (2, 1, 3, 0)
SP = 16


def dot(a, b):
    return jnp.dot(a, b, preferred_element_type=F32)


def dot_t(a, b):
    return lax.dot_general(a, b, (((1,), (1,)), ((), ())), preferred_element_type=F32)


def dot_exact(a, b):
    return jnp.dot(a, b, preferred_element_type=F32, precision=lax.Precision.HIGHEST)


def softplus(v):
    return jnp.maximum(v, 0.0) + jnp.log1p(jnp.exp(-jnp.abs(v)))


def kernel(
    x_hbm, xnew_hbm, wx_hbm, wb_hbm, wc_hbm, wdt_hbm, wz_hbm,
    cw_hbm, cb_hbm, dtb_hbm, alog_hbm, dskip_hbm, ng_hbm,
    st_out, ro_out,
    x_ref, xnew_ref, wx_ref, wb_ref, wc_ref, wdt_ref, wz_ref,
    cw_ref, cb_ref, dtb_ref, alog_ref, dskip_ref, ng_ref,
    pre_refs, key_refs, sc_refs, wg_ref, fac_ref,
    edge_tx, halo_rx, tail_rx, tot_tx, tot_rx,
    tx1, rx1, tx2, rx2,
    in_sems, w_sems,
    halo_s, halo_r, tail_s, tail_r, tot_s, tot_r, s1_s, s1_r, s2_s, s2_r,
):
    scope = jax.named_scope
    i = lax.axis_index("sp")
    j = lax.axis_index("tp")
    zp, xp = i // 4, i % 4
    yp, cp = j // 2, j % 2
    other = 1 - cp

    def pair(t):
        return (yp + OFFS[t]) % 4

    def load(src, dst, n):
        return pltpu.make_async_copy(src, dst, in_sems.at[n])

    first_loads = [
        load(x_hbm.at[0], x_ref.at[pl.ds(0, T), :], 0),
        load(x_hbm.at[1], x_ref.at[pl.ds(T, T), :], 1),
        load(wdt_hbm, wdt_ref, 2),
        load(dtb_hbm, dtb_ref, 3),
        load(alog_hbm, alog_ref, 4),
    ]
    conv_loads = [load(cw_hbm, cw_ref, 5), load(cb_hbm, cb_ref, 6)]
    last_loads = [
        load(xnew_hbm, xnew_ref, 7),
        load(dskip_hbm, dskip_ref, 8),
        load(ng_hbm, ng_ref, 9),
        load(wz_hbm, wz_ref, 10),
        load(wc_hbm.at[:, pl.ds(pl.multiple_of(j * N, N), N)], wc_ref, 11),
    ]

    def w_copy(t):
        q = pair(t)
        kcols = pl.ds(pl.multiple_of(q * 256, 256), 256)
        vcols = pl.ds(pl.multiple_of(q * 512, 512), 512)
        return [
            pltpu.make_async_copy(wb_hbm.at[:, kcols], wb_ref.at[:, kcols], w_sems.at[t, 0]),
            pltpu.make_async_copy(wx_hbm.at[:, vcols], wx_ref.at[:, vcols], w_sems.at[t, 1]),
        ]

    for c in first_loads + w_copy(0):
        c.start()

    bar = pltpu.get_barrier_semaphore()

    def sig(sp, tp):
        pl.semaphore_signal(bar, inc=1, device_id=(sp, tp), device_id_type=MESH)

    for d in range(1, SP):
        sig((i + d) % SP, j)

    @pl.when(cp != xp // 2)
    def _():
        for d in range(4):
            sig(zp * 4 + d, 2 * yp + other)

    for d in range(4):
        @pl.when((d != zp) | (yp != zp))
        def _():
            sig(d * 4 + xp, 2 * zp + cp)

    tail_tp = i // 2

    @pl.when((i != SP - 1) | (j != tail_tp))
    def _():
        sig(SP - 1, tail_tp)

    for c in conv_loads:
        c.start()

    with scope("xwait"):
        for c in first_loads:
            c.wait()
    for t in range(1, 4):
        for c in w_copy(t):
            c.start()
    for c in last_loads:
        c.start()
    lo = x_ref[T - 16:T, :].astype(F32)[13:16]
    hi = x_ref[2 * T - 16:2 * T, :].astype(F32)[13:16]
    edge_tx[...] = jnp.concatenate([lo, hi, jnp.zeros((2, D), F32)], axis=0).astype(BF)

    raw = dot_t(x_ref[0:2 * T, :], wdt_ref[...])
    steps = softplus(raw + dtb_ref[...])
    tot_tx[...] = jnp.zeros_like(tot_tx)
    rates = -jnp.exp(alog_ref[...])
    for s in range(2):
        tot_tx[s:s + 1, 0:H] = jnp.sum(steps[T * s:T * (s + 1)], axis=0, keepdims=True)

    s1_self = (cp == xp // 2)
    arrivals = 15 + 2 + 4 - jnp.where(zp == yp, 1, 0)
    arrivals = arrivals + jnp.where(i == SP - 1, 16 - jnp.where(j == 7, 1, 0), 0)
    with scope("barrier"):
        pl.semaphore_wait(bar, arrivals)

    halo_copy = pltpu.make_async_remote_copy(
        edge_tx, halo_rx, halo_s, halo_r, device_id=((i + 1) % SP, j), device_id_type=MESH
    )

    @pl.when(i < SP - 1)
    def _():
        halo_copy.start()

    def tot_copy(d):
        return pltpu.make_async_remote_copy(
            tot_tx, tot_rx.at[i], tot_s.at[d], tot_r.at[i],
            device_id=((i + d) % SP, j), device_id_type=MESH,
        )

    for d in range(1, SP):
        tot_copy(d).start()

    with scope("w0wait"):
        for c in w_copy(0):
            c.wait()
        for c in conv_loads:
            c.wait()

    upper = (
        lax.broadcasted_iota(jnp.int32, (T, T), 1) > lax.broadcasted_iota(jnp.int32, (T, T), 0)
    ).astype(F32).astype(BF)

    def weights(s):
        own = steps[T * s:T * (s + 1)]
        high = own.astype(BF)
        low = (own - high.astype(F32)).astype(BF)
        rest = dot(upper, high) + dot(upper, low)
        weight = jnp.exp(rates * rest) * own
        for g in range(G):
            wg_ref[g, T * s:T * (s + 1), 0:R] = weight[:, R * g:R * (g + 1)]

    def w_slice(t, u):
        q = pair(t)
        if u == 0:
            return wb_ref[:, pl.ds(pl.multiple_of(q * 256, 256), 256)]
        return wx_ref[:, pl.ds(pl.multiple_of(q * 512 + 256 * (u - 1), 256), 256)]

    def put_halo(pre, rows):
        for c in range(2):
            pre[c, 5:8, :] = rows[0:3, 128 * c:128 * (c + 1)]
            pre[c, T + 13:T + 16, :] = rows[3:6, 128 * c:128 * (c + 1)]

    def pre_of(n):
        return pre_refs[n % 6]

    def proj(n, s):
        t, u = n // 3, n % 3
        pre = pre_of(n)
        rows = T + (16 if t > 0 and s == 1 else 0)
        res = dot(x_ref[T * s:T * s + rows, :], w_slice(t, u))
        for c in range(2):
            pre[c, (T + 8) * s + 8:(T + 8) * (s + 1), :] = res[0:T, 128 * c:128 * (c + 1)]
        if t > 0 and s == 1:
            put_halo(pre, res[T:T + 8])

    for n in range(3):
        for s in range(2):
            proj(n, s)
            if n == 1:
                weights(s)

    with scope("halowait"):
        @pl.when(i > 0)
        def _():
            halo_copy.wait_recv()
    halo = jnp.where(i > 0, halo_rx[...].astype(F32), 0.0)
    x_ref[2 * T:2 * T + 16, :] = jnp.concatenate([halo, jnp.zeros((8, D), F32)], axis=0).astype(BF)
    for u in range(3):
        put_halo(pre_of(u), dot(x_ref[2 * T:2 * T + 16, :], w_slice(0, u))[0:8])

    lane = lax.broadcasted_iota(jnp.int32, (128, 128), 1)

    def conv(pre, s, c, r, off):
        cols = pl.ds(pl.multiple_of(off + 128 * c, 128), 128)
        taps = cw_ref[:, cols] * 0.5
        acc = cb_ref[:, cols] * 0.5 + taps[3:4] * pre[c, pl.ds((T + 8) * s + 8 + r, 128), :]
        for k in range(3):
            acc = acc + taps[k:k + 1] * pre[c, pl.ds((T + 8) * s + 5 + k + r, 128), :]
        return acc + acc * jnp.tanh(acc)

    def post_keys(t, s):
        q = pair(t)
        for c in range(2):
            for r in range(0, T, 128):
                out = conv(pre_of(3 * t), s, c, r, H * P_SIZE + q * 256)
                key_refs[t % 2][T * s + r:T * s + r + 128, 128 * c:128 * (c + 1)] = out.astype(BF)

    def post_values(t, b, s):
        g = 2 * pair(t) + b
        for c in range(2):
            for r in range(0, T, 128):
                out = conv(pre_of(3 * t + 1 + b), s, c, r, g * 256)
                w = wg_ref[g, pl.ds(T * s + r, 128), 0:R]
                w = jnp.where(lane < P_SIZE, w[:, 2 * c:2 * c + 1], w[:, 2 * c + 1:2 * c + 2])
                sc_refs[b][T * s + r:T * s + r + 128, 128 * c:128 * (c + 1)] = (out * w).astype(BF)

    def post(n, s):
        if n % 3 == 0:
            post_keys(n // 3, s)
        else:
            post_values(n // 3, n % 3 - 1, s)

    def s1_copy(t, a, b):
        n = 4 * t + 2 * a + b
        return pltpu.make_async_remote_copy(
            tx1.at[n], rx1.at[t, xp], s1_s.at[n], s1_r.at[t, xp],
            device_id=(zp * 4 + 2 * cp + a, 2 * yp + b), device_id_type=MESH,
        )

    def s1_own(a, b):
        return (xp == 2 * cp + a) & (cp == b)

    def contract(t, a, b):
        g = 2 * pair(t) + b
        keys = key_refs[t % 2][T * a:T * (a + 1), 128 * b:128 * (b + 1)]
        term = lax.dot_general(
            keys, sc_refs[b][T * a:T * (a + 1), :], (((0,), (0,)), ((), ())),
            preferred_element_type=F32,
        )
        term = term * fac_ref[g, a:a + 1, :]
        tx1[4 * t + 2 * a + b] = term.astype(BF)

    def send1(t, a, b):
        @pl.when(jnp.logical_not(s1_own(a, b)))
        def _():
            s1_copy(t, a, b).start()

        @pl.when(s1_own(a, b))
        def _():
            rx1[t, xp] = tx1[4 * t + 2 * a + b]

    def s2_copy(t):
        return pltpu.make_async_remote_copy(
            tx2.at[t], rx2.at[zp], s2_s.at[t], s2_r.at[zp],
            device_id=(yp * 4 + xp, 2 * pair(t) + cp), device_id_type=MESH,
        )

    def stage2(t):
        with scope("s1wait"):
            for d in range(4):
                @pl.when(jnp.logical_not((d == xp) & s1_self))
                def _():
                    pltpu.make_async_remote_copy(
                        tx1.at[0], rx1.at[t, d], s1_s.at[0], s1_r.at[t, d],
                        device_id=(i, j), device_id_type=MESH,
                    ).wait_recv()
        acc = rx1[t, 0].astype(F32)
        for d in range(1, 4):
            acc = acc + rx1[t, d].astype(F32)
        tx2[t] = acc.astype(BF)
        if OFFS[t] == 0:
            @pl.when(yp != zp)
            def _():
                s2_copy(t).start()

            @pl.when(yp == zp)
            def _():
                rx2[zp] = tx2[t]
        else:
            s2_copy(t).start()

    def factors():
        with scope("totwait"):
            for d in range(1, SP):
                src = (i + SP - d) % SP
                pltpu.make_async_remote_copy(
                    tot_tx, tot_rx.at[src], tot_s.at[d], tot_r.at[src],
                    device_id=((i + d) % SP, j), device_id_type=MESH,
                ).wait_recv()
        later = jnp.zeros((2, 128), F32)
        for d in range(SP):
            later = later + jnp.where(i < d, tot_rx[d], 0.0)
        factor = jnp.exp(rates * later[:, 0:H])
        spread = (
            lax.broadcasted_iota(jnp.int32, (H, H * P_SIZE), 1) // P_SIZE
            == lax.broadcasted_iota(jnp.int32, (H, H * P_SIZE), 0)
        ).astype(F32)
        wide = dot_exact(jnp.concatenate([factor, jnp.zeros((6, H), F32)], axis=0), spread)
        for g in range(G):
            fac_ref[g] = wide[:, 256 * g:256 * (g + 1)]

    def tail_copy(n):
        return pltpu.make_async_remote_copy(
            edge_tx, tail_rx, tail_s.at[n], tail_r,
            device_id=(2 * j + n % 2, n // 2), device_id_type=MESH,
        )

    def tail_self(n):
        return (j == 7) & (2 * j + n % 2 == i) & (n // 2 == j)

    def send_tails():
        @pl.when(i == SP - 1)
        def _():
            for n in range(16):
                @pl.when(jnp.logical_not(tail_self(n)))
                def _():
                    tail_copy(n).start()

        @pl.when((i == SP - 1) & (j == 7))
        def _():
            tail_rx[...] = edge_tx[...]

    slots = (
        (3, (0,)), (4, (1,)), (5, (2,)), (6, (3,)), (7, (4,)), (8, (5, 6)),
        (9, (7,)), (10, (8, 9)), (11, (10,)), (None, (11,)),
    )
    for k, (p, posts) in enumerate(slots):
        if p is not None and p % 3 == 0:
            with scope("wwait"):
                for c in w_copy(p // 3):
                    c.wait()
        with scope("slot"):
            for s in range(2):
                if p is not None:
                    proj(p, s)
                for n in posts:
                    post(n, s)
        if k == 1:
            factors()
        for n in posts:
            if n % 3:
                t, b = n // 3, n % 3 - 1
                for a in range(2):
                    contract(t, a, b)
                for a in range(2):
                    send1(t, a, b)
        if k == 3:
            send_tails()
        if k == 6:
            stage2(0)
        if k == 8:
            stage2(1)

    with scope("tailwait"):
        for c in last_loads:
            c.wait()

        @pl.when(jnp.logical_not((i == SP - 1) & (j == 7)))
        def _():
            tail_copy(0).wait_recv()

    ext = jnp.concatenate(
        [tail_rx[...].astype(F32), jnp.broadcast_to(xnew_ref[...].astype(F32), (8, D))], axis=0
    ).astype(BF)
    a_own = i % 2

    def fresh(w, off, width):
        res = dot(ext, w)
        cols = pl.ds(pl.multiple_of(off, 128), width)
        taps = cw_ref[:, cols] * 0.5
        acc = cb_ref[:, cols] * 0.5 + taps[3:4] * res[8:9]
        for k in range(3):
            acc = acc + taps[k:k + 1] * jnp.where(a_own == 0, res[k:k + 1], res[3 + k:4 + k])
        return acc + acc * jnp.tanh(acc)

    values = fresh(wx_ref[:, pl.ds(pl.multiple_of(j * 256, 256), 256)], j * 256, 256)
    keys = fresh(wb_ref[:, pl.ds(pl.multiple_of(j * N, N), N)], H * P_SIZE + j * N, N)
    query = fresh(wc_ref[...], H * P_SIZE + G * N + j * N, N)
    gate = dot(ext, wz_ref[...])[8:9]
    new_raw = dot_t(ext, wdt_ref[...])[8:9]
    new_steps = softplus(new_raw + dtb_ref[...])
    row = lax.broadcasted_iota(jnp.int32, (8, H), 0)
    packed = jnp.where(
        row == 0, new_steps, jnp.where(row == 1, jnp.exp(rates * new_steps), dskip_ref[...])
    )
    own_spread = (
        lax.broadcasted_iota(jnp.int32, (H, 256), 1) // P_SIZE + R * j
        == lax.broadcasted_iota(jnp.int32, (H, 256), 0)
    ).astype(F32)
    per_lane = dot_exact(packed, own_spread)
    step_row, decay_row, skip_row = per_lane[0:1], per_lane[1:2], per_lane[2:3]
    inner = jnp.sum(query * keys, axis=1, keepdims=True)
    direct = (step_row * inner + skip_row) * values
    gate = gate * jax.nn.sigmoid(gate)

    stage2(2)
    stage2(3)

    with scope("s2wait"):
        for d in range(4):
            @pl.when(jnp.logical_not((d == zp) & (yp == zp)))
            def _():
                pltpu.make_async_remote_copy(
                    tx2.at[0], rx2.at[d], s2_s.at[0], s2_r.at[d],
                    device_id=(i, j), device_id_type=MESH,
                ).wait_recv()
    state = rx2[0].astype(F32)
    for d in range(1, 4):
        state = state + rx2[d].astype(F32)
    st_out[0] = state.T.astype(BF).reshape(R, P_SIZE, N)
    held = dot_exact(jnp.broadcast_to(query, (8, N)), state)[0:1]
    gated = (decay_row * held + direct) * gate
    ms = jnp.sum(gated * gated, axis=1, keepdims=True) * (1.0 / 256)
    normed = gated * lax.rsqrt(ms + eps)
    head = lax.broadcasted_iota(jnp.int32, (R, 256), 0)
    chan = lax.broadcasted_iota(jnp.int32, (R, 256), 1) // P_SIZE
    split = jnp.where(head == chan, normed, 0.0)
    split = split[:, 0:128] + split[:, 128:256]
    split = split[:, 0:P_SIZE] + split[:, P_SIZE:128]
    ro_out[0] = (split * ng_ref[...]).astype(BF)

    with scope("drain"):
        @pl.when(i < SP - 1)
        def _():
            halo_copy.wait_send()

        for d in range(1, SP):
            tot_copy(d).wait_send()

        @pl.when(i == SP - 1)
        def _():
            for n in range(16):
                @pl.when(jnp.logical_not(tail_self(n)))
                def _():
                    tail_copy(n).wait_send()

        for t in range(4):
            for a in range(2):
                for b in range(2):
                    @pl.when(jnp.logical_not(s1_own(a, b)))
                    def _():
                        s1_copy(t, a, b).wait_send()
            if OFFS[t] == 0:
                @pl.when(yp != zp)
                def _():
                    s2_copy(t).wait_send()
            else:
                s2_copy(t).wait_send()


def per_device(
    x_in, x_new, w_x, w_b, w_c, w_dt, w_z, conv_w, conv_b, dt_bias, a_log, d_skip, norm_g
):
    hbm = pl.BlockSpec(memory_space=pl.ANY)
    vmem = pl.BlockSpec(memory_space=pltpu.VMEM)
    dma = pltpu.SemaphoreType.DMA
    return pl.pallas_call(
        kernel,
        out_shape=(
            jax.ShapeDtypeStruct((1, R, P_SIZE, N), BF),
            jax.ShapeDtypeStruct((1, R, P_SIZE), BF),
        ),
        in_specs=[hbm] * 13,
        out_specs=(vmem, vmem),
        scratch_shapes=[
            pltpu.VMEM((2 * T + 16, D), BF),
            pltpu.VMEM((1, D), BF),
            pltpu.VMEM((D, H * P_SIZE), BF),
            pltpu.VMEM((D, G * N), BF),
            pltpu.VMEM((D, N), BF),
            pltpu.VMEM((H, D), BF),
            pltpu.VMEM((D, 256), BF),
            pltpu.VMEM((KW, 4096), F32),
            pltpu.VMEM((1, 4096), F32),
            pltpu.VMEM((1, H), F32),
            pltpu.VMEM((1, H), F32),
            pltpu.VMEM((1, H), F32),
            pltpu.VMEM((R, P_SIZE), F32),
            [pltpu.VMEM((2, 2 * (T + 8), 128), F32) for _ in range(6)],
            [pltpu.VMEM((2 * T, 256), BF) for _ in range(2)],
            [pltpu.VMEM((2 * T, 256), BF) for _ in range(2)],
            pltpu.VMEM((G, 2 * T, 128), F32),
            pltpu.VMEM((G, 8, 256), F32),
            pltpu.VMEM((8, D), BF),
            pltpu.VMEM((8, D), BF),
            pltpu.VMEM((8, D), BF),
            pltpu.VMEM((2, 128), F32),
            pltpu.VMEM((SP, 2, 128), F32),
            pltpu.VMEM((16, N, 256), BF),
            pltpu.VMEM((4, 4, N, 256), BF),
            pltpu.VMEM((4, N, 256), BF),
            pltpu.VMEM((4, N, 256), BF),
            dma((12,)),
            dma((4, 2)),
            dma,
            dma,
            dma((16,)),
            dma,
            dma((SP,)),
            dma((SP,)),
            dma((16,)),
            dma((4, 4)),
            dma((4,)),
            dma((4,)),
        ],
        compiler_params=pltpu.CompilerParams(
            collective_id=0, has_side_effects=True, vmem_limit_bytes=60 * 1024 * 1024
        ),
    )(
        x_in, x_new, w_x, w_b, w_c, w_dt.T, w_z, conv_w,
        conv_b.reshape(1, -1), dt_bias.reshape(1, -1), a_log.reshape(1, -1),
        d_skip.reshape(1, -1), norm_g,
    )


def solution(mesh):
    return jax.shard_map(
        per_device,
        mesh=mesh,
        in_specs=(
            P("tp", "sp", None),
            P("sp", None),
            P(),
            P(),
            P(),
            P(),
            P(None, "tp"),
            P(),
            P(),
            P(),
            P(),
            P(),
            P("tp", None),
        ),
        out_specs=(P("sp", "tp", None, None), P("sp", "tp", None)),
        check_vma=False,
    )
```

time: 50.7 us -> 43.1 us (0.85)
  Pallas kernels: 45.2 us -> 39.1 us
  local copies, waits for them, and re-layouts: 4.6 us -> 2.67 us
    pallas_call x1, Pallas kernels: 45.2 us -> 39.1 us  [per_device(): pl.pallas_call(kernel, out_shape=(jax.ShapeDtypeStruct((1, R, P_SIZE, N),...]
    unnamed x3 -> x2, local copies, waits for them, and re-layouts: 4.6 us -> 2.67 us
where the time goes in v2:
time: 43.1 us; the launch traced here: 42.4 us
  Pallas kernels  39.1 us (91%)
  local copies, waits for them, and re-layouts  2.67 us (6%)
  between operations  0.64 us (1%)
    pallas_call x1, Pallas kernels, per_device(): pl.pallas_call(kernel, out_shape=(jax.ShapeDtypeStruct((1, R, P_SIZE, N),...  39.1 us
    unnamed x2, local copies, waits for them, and re-layouts  2.67 us

profile of v2, /device:TPU:1, one launch (start us, length us, event | category | flops | bytes accessed | tf_op | source)
XLA Modules:
  0.0 42.4 jit_solution(18238126701969821413)
XLA Ops:
  0.6 39.1 %shard_map.140 = (bf16[1,4,64,128]{3,2,1,0:T(8,128)(2,1)}, bf16[1,4,64]{2,1,0:T(4,128)(2,1)}) custom-call(bf16[2,384,2048]{2,1,0:T(8,128)(2,1)} %x_hbm.1, bf16[1,2048]{1,0:T(2,128)(2,1)} %xnew_hbm.1, bf16[2048,2048]{1,0:T(8,128)(2,1)} %wx_hbm.1, bf16[2048,1024]{1,0:T(8,128)(2,1)} %wb_hbm.1, bf16[2048,1024]{1,0:T(8,128)(2,1)} %wc_hbm.1, ...), custom_call_target="tpu_custom_call" | custom-call | tf_op jit(solution)/shard_map/pallas_call | solution.py:486
  39.7 1.5 %copy.17 = bf16[1,4,64,128]{3,2,1,0:T(8,128)(2,1)} copy(bf16[1,4,64,128]{3,2,1,0:T(8,128)(2,1)} %get-tuple-element.4) | data formatting | bytes 131072
  41.2 1.2 %copy.18 = bf16[1,4,64]{2,1,0:T(4,128)(2,1)} copy(bf16[1,4,64]{2,1,0:T(4,128)(2,1)} %get-tuple-element.5) | data formatting | bytes 1024

commit v3 on v2

--- a/solution.py
+++ b/solution.py
@@ -17,7 +17,7 @@
 MESH = pl.DeviceIdType.MESH
 BF = jnp.bfloat16
 F32 = jnp.float32
-OFFS = (2, 1, 3, 0)
+OFFS = (0, 1, 3, 2)
 SP = 16
 
 
@@ -57,7 +57,7 @@
     other = 1 - cp
 
     def pair(t):
-        return (yp + OFFS[t]) % 4
+        return (2 * yp + 4 - zp + OFFS[t]) % 4
 
     def load(src, dst, n):
         return pltpu.make_async_copy(src, dst, in_sems.at[n])
@@ -129,13 +129,6 @@
     hi = x_ref[2 * T - 16:2 * T, :].astype(F32)[13:16]
     edge_tx[...] = jnp.concatenate([lo, hi, jnp.zeros((2, D), F32)], axis=0).astype(BF)
 
-    raw = dot_t(x_ref[0:2 * T, :], wdt_ref[...])
-    steps = softplus(raw + dtb_ref[...])
-    tot_tx[...] = jnp.zeros_like(tot_tx)
-    rates = -jnp.exp(alog_ref[...])
-    for s in range(2):
-        tot_tx[s:s + 1, 0:H] = jnp.sum(steps[T * s:T * (s + 1)], axis=0, keepdims=True)
-
     s1_self = (cp == xp // 2)
     arrivals = 15 + 2 + 4 - jnp.where(zp == yp, 1, 0)
     arrivals = arrivals + jnp.where(i == SP - 1, 16 - jnp.where(j == 7, 1, 0), 0)
@@ -150,20 +143,16 @@
     def _():
         halo_copy.start()
 
+    raw = dot_t(x_ref[0:2 * T, :], wdt_ref[...])
+    steps = softplus(raw + dtb_ref[...])
+    tot_tx[...] = jnp.zeros_like(tot_tx)
+    rates = -jnp.exp(alog_ref[...])
+
     def tot_copy(d):
         return pltpu.make_async_remote_copy(
             tot_tx, tot_rx.at[i], tot_s.at[d], tot_r.at[i],
             device_id=((i + d) % SP, j), device_id_type=MESH,
         )
-
-    for d in range(1, SP):
-        tot_copy(d).start()
-
-    with scope("w0wait"):
-        for c in w_copy(0):
-            c.wait()
-        for c in conv_loads:
-            c.wait()
 
     upper = (
         lax.broadcasted_iota(jnp.int32, (T, T), 1) > lax.broadcasted_iota(jnp.int32, (T, T), 0)
@@ -195,27 +184,38 @@
     def proj(n, s):
         t, u = n // 3, n % 3
         pre = pre_of(n)
-        rows = T + (16 if t > 0 and s == 1 else 0)
+        rows = T + 16 * s
         res = dot(x_ref[T * s:T * s + rows, :], w_slice(t, u))
         for c in range(2):
             pre[c, (T + 8) * s + 8:(T + 8) * (s + 1), :] = res[0:T, 128 * c:128 * (c + 1)]
-        if t > 0 and s == 1:
+        if s == 1:
             put_halo(pre, res[T:T + 8])
 
-    for n in range(3):
-        for s in range(2):
-            proj(n, s)
-            if n == 1:
-                weights(s)
+    with scope("w0wait"):
+        for c in w_copy(0) + conv_loads:
+            c.wait()
+
+    proj(0, 0)
+    for s in range(2):
+        tot_tx[s:s + 1, 0:H] = jnp.sum(steps[T * s:T * (s + 1)], axis=0, keepdims=True)
+    for d in range(1, SP):
+        tot_copy(d).start()
+    proj(1, 0)
+    weights(0)
+    proj(2, 0)
 
     with scope("halowait"):
         @pl.when(i > 0)
         def _():
             halo_copy.wait_recv()
+        for c in w_copy(1):
+            c.wait()
     halo = jnp.where(i > 0, halo_rx[...].astype(F32), 0.0)
     x_ref[2 * T:2 * T + 16, :] = jnp.concatenate([halo, jnp.zeros((8, D), F32)], axis=0).astype(BF)
-    for u in range(3):
-        put_halo(pre_of(u), dot(x_ref[2 * T:2 * T + 16, :], w_slice(0, u))[0:8])
+    proj(0, 1)
+    weights(1)
+    proj(1, 1)
+    proj(2, 1)
 
     lane = lax.broadcasted_iota(jnp.int32, (128, 128), 1)
 
@@ -354,7 +354,7 @@
         (9, (7,)), (10, (8, 9)), (11, (10,)), (None, (11,)),
     )
     for k, (p, posts) in enumerate(slots):
-        if p is not None and p % 3 == 0:
+        if p is not None and p % 3 == 0 and p > 3:
             with scope("wwait"):
                 for c in w_copy(p // 3):
                     c.wait()
@@ -486,8 +486,8 @@
     return pl.pallas_call(
         kernel,
         out_shape=(
-            jax.ShapeDtypeStruct((1, R, P_SIZE, N), BF),
-            jax.ShapeDtypeStruct((1, R, P_SIZE), BF),
+            pltpu.VMEM((1, R, P_SIZE, N), BF),
+            pltpu.VMEM((1, R, P_SIZE), BF),
         ),
         in_specs=[hbm] * 13,
         out_specs=(vmem, vmem),

time: 43.1 us -> 41.1 us (0.954)
  the two profiles are of different devices: /device:TPU:1 before, /device:TPU:27 now
where the time goes in v3:
time: 41.1 us; the launch traced here: 41 us
  Pallas kernels  39.2 us (95%)
  local copies, waits for them, and re-layouts  1.19 us (3%)
  between operations  0.64 us (2%)
    pallas_call x1, Pallas kernels, per_device(): pl.pallas_call(kernel, out_shape=(pltpu.VMEM((1, R, P_SIZE, N), BF), pltp...  39.2 us
    unnamed x2, local copies, waits for them, and re-layouts  1.19 us

profile of v3, /device:TPU:27, one launch (start us, length us, event | category | flops | bytes accessed | tf_op | source)
XLA Modules:
  0.0 41.0 jit_solution(14660113485305409184)
XLA Ops:
  0.6 39.2 %shard_map.140 = (bf16[1,4,64,128]{3,2,1,0:T(8,128)(2,1)S(1)}, bf16[1,4,64]{2,1,0:T(4,128)(2,1)S(1)}) custom-call(bf16[2,384,2048]{2,1,0:T(8,128)(2,1)} %x_hbm.1, bf16[1,2048]{1,0:T(2,128)(2,1)} %xnew_hbm.1, bf16[2048,2048]{1,0:T(8,128)(2,1)} %wx_hbm.1, bf16[2048,1024]{1,0:T(8,128)(2,1)} %wb_hbm.1, bf16[2048,1024]{1,0:T(8,128)(2,1)} %wc_hbm.1, ...), custom_call_target="tpu_custom_call" | custom-call | tf_op jit(solution)/shard_map/pallas_call | solution.py:486
  39.8 0.6 %copy.17 = bf16[1,4,64,128]{3,2,1,0:T(8,128)(2,1)} copy(bf16[1,4,64,128]{3,2,1,0:T(8,128)(2,1)S(1)} %get-tuple-element.2) | data formatting | bytes 131072
  40.4 0.6 %copy.18 = bf16[1,4,64]{2,1,0:T(4,128)(2,1)} copy(bf16[1,4,64]{2,1,0:T(4,128)(2,1)S(1)} %get-tuple-element.3) | data formatting | bytes 1024

commit v4 on v3

--- a/solution.py
+++ b/solution.py
@@ -44,7 +44,7 @@
     x_ref, xnew_ref, wx_ref, wb_ref, wc_ref, wdt_ref, wz_ref,
     cw_ref, cb_ref, dtb_ref, alog_ref, dskip_ref, ng_ref,
     pre_refs, key_refs, sc_refs, wg_ref, fac_ref,
-    edge_tx, halo_rx, tail_rx, tot_tx, tot_rx,
+    edge_tx, tail_tx, halo_rx, tail_rx, tot_tx, tot_rx,
     tx1, rx1, tx2, rx2,
     in_sems, w_sems,
     halo_s, halo_r, tail_s, tail_r, tot_s, tot_r, s1_s, s1_r, s2_s, s2_r,
@@ -63,11 +63,11 @@
         return pltpu.make_async_copy(src, dst, in_sems.at[n])
 
     first_loads = [
-        load(x_hbm.at[0], x_ref.at[pl.ds(0, T), :], 0),
-        load(x_hbm.at[1], x_ref.at[pl.ds(T, T), :], 1),
+        load(x_hbm.at[0], x_ref.at[pl.ds(16, T), :], 0),
         load(wdt_hbm, wdt_ref, 2),
         load(dtb_hbm, dtb_ref, 3),
         load(alog_hbm, alog_ref, 4),
+        load(x_hbm.at[1], x_ref.at[pl.ds(16 + T, T), :], 1),
     ]
     conv_loads = [load(cw_hbm, cw_ref, 5), load(cb_hbm, cb_ref, 6)]
     last_loads = [
@@ -118,15 +118,18 @@
         c.start()
 
     with scope("xwait"):
-        for c in first_loads:
+        for c in first_loads[:-1]:
             c.wait()
+    raw0 = dot_t(x_ref[16:16 + T, :], wdt_ref[...])
+    with scope("xwait"):
+        first_loads[-1].wait()
     for t in range(1, 4):
         for c in w_copy(t):
             c.start()
     for c in last_loads:
         c.start()
-    lo = x_ref[T - 16:T, :].astype(F32)[13:16]
-    hi = x_ref[2 * T - 16:2 * T, :].astype(F32)[13:16]
+    lo = x_ref[T:T + 16, :].astype(F32)[13:16]
+    hi = x_ref[2 * T:2 * T + 16, :].astype(F32)[13:16]
     edge_tx[...] = jnp.concatenate([lo, hi, jnp.zeros((2, D), F32)], axis=0).astype(BF)
 
     s1_self = (cp == xp // 2)
@@ -143,7 +146,29 @@
     def _():
         halo_copy.start()
 
-    raw = dot_t(x_ref[0:2 * T, :], wdt_ref[...])
+    def tail_copy(n):
+        return pltpu.make_async_remote_copy(
+            tail_tx.at[n % 2], tail_rx, tail_s.at[n], tail_r,
+            device_id=(2 * j + n % 2, n // 2), device_id_type=MESH,
+        )
+
+    def tail_self(n):
+        return (j == 7) & (2 * j + n % 2 == i) & (n // 2 == j)
+
+    @pl.when(i == SP - 1)
+    def _():
+        tail_tx[0] = jnp.concatenate([lo, lo[0:1]], axis=0).astype(BF)
+        tail_tx[1] = jnp.concatenate([hi, hi[0:1]], axis=0).astype(BF)
+        for n in range(16):
+            @pl.when(jnp.logical_not(tail_self(n)))
+            def _():
+                tail_copy(n).start()
+
+    @pl.when((i == SP - 1) & (j == 7))
+    def _():
+        tail_rx[...] = tail_tx[1]
+
+    raw = jnp.concatenate([raw0, dot_t(x_ref[16 + T:16 + 2 * T, :], wdt_ref[...])], axis=0)
     steps = softplus(raw + dtb_ref[...])
     tot_tx[...] = jnp.zeros_like(tot_tx)
     rates = -jnp.exp(alog_ref[...])
@@ -182,27 +207,27 @@
         return pre_refs[n % 6]
 
     def proj(n, s):
-        t, u = n // 3, n % 3
         pre = pre_of(n)
-        rows = T + 16 * s
-        res = dot(x_ref[T * s:T * s + rows, :], w_slice(t, u))
+        lead = 16 * (1 - s)
+        start = (16 + T) * s
+        res = dot(x_ref[start:start + T + lead, :], w_slice(n // 3, n % 3))
         for c in range(2):
-            pre[c, (T + 8) * s + 8:(T + 8) * (s + 1), :] = res[0:T, 128 * c:128 * (c + 1)]
-        if s == 1:
-            put_halo(pre, res[T:T + 8])
+            pre[c, (T + 8) * s + 8:(T + 8) * (s + 1), :] = res[lead:lead + T, 128 * c:128 * (c + 1)]
+        if s == 0:
+            put_halo(pre, res[0:8])
 
     with scope("w0wait"):
         for c in w_copy(0) + conv_loads:
             c.wait()
 
-    proj(0, 0)
+    proj(0, 1)
     for s in range(2):
         tot_tx[s:s + 1, 0:H] = jnp.sum(steps[T * s:T * (s + 1)], axis=0, keepdims=True)
     for d in range(1, SP):
         tot_copy(d).start()
-    proj(1, 0)
+    proj(1, 1)
     weights(0)
-    proj(2, 0)
+    proj(2, 1)
 
     with scope("halowait"):
         @pl.when(i > 0)
@@ -211,11 +236,11 @@
         for c in w_copy(1):
             c.wait()
     halo = jnp.where(i > 0, halo_rx[...].astype(F32), 0.0)
-    x_ref[2 * T:2 * T + 16, :] = jnp.concatenate([halo, jnp.zeros((8, D), F32)], axis=0).astype(BF)
-    proj(0, 1)
+    x_ref[0:16, :] = jnp.concatenate([halo, jnp.zeros((8, D), F32)], axis=0).astype(BF)
+    proj(0, 0)
     weights(1)
-    proj(1, 1)
-    proj(2, 1)
+    proj(1, 0)
+    proj(2, 0)
 
     lane = lax.broadcasted_iota(jnp.int32, (128, 128), 1)
 
@@ -328,53 +353,44 @@
         for g in range(G):
             fac_ref[g] = wide[:, 256 * g:256 * (g + 1)]
 
-    def tail_copy(n):
-        return pltpu.make_async_remote_copy(
-            edge_tx, tail_rx, tail_s.at[n], tail_r,
-            device_id=(2 * j + n % 2, n // 2), device_id_type=MESH,
-        )
-
-    def tail_self(n):
-        return (j == 7) & (2 * j + n % 2 == i) & (n // 2 == j)
-
-    def send_tails():
-        @pl.when(i == SP - 1)
-        def _():
-            for n in range(16):
-                @pl.when(jnp.logical_not(tail_self(n)))
-                def _():
-                    tail_copy(n).start()
-
-        @pl.when((i == SP - 1) & (j == 7))
-        def _():
-            tail_rx[...] = edge_tx[...]
-
     slots = (
-        (3, (0,)), (4, (1,)), (5, (2,)), (6, (3,)), (7, (4,)), (8, (5, 6)),
-        (9, (7,)), (10, (8, 9)), (11, (10,)), (None, (11,)),
+        ("3a3b", "0a0b"), ("4a4b", "1a1b"), ("5a5b", "2a2b3a"), ("6a6b", "3b4a4b"),
+        ("7a7b", "5a5b6a"), ("8a8b", "6b7a7b"), ("9a9b", "8a8b9a"), ("10a10b", "9b10a"),
+        ("11a", "10b"), ("11b", "11a11b"),
     )
-    for k, (p, posts) in enumerate(slots):
-        if p is not None and p % 3 == 0 and p > 3:
+
+    def halves(text):
+        out, num = [], ""
+        for ch in text:
+            if ch in "ab":
+                out.append((int(num), "ab".index(ch)))
+                num = ""
+            else:
+                num += ch
+        return out
+
+    for k, (projs, posts) in enumerate(slots):
+        projs, posts = halves(projs), halves(posts)
+        n = projs[0][0]
+        if projs[0][1] == 0 and n % 3 == 0 and n > 3:
             with scope("wwait"):
-                for c in w_copy(p // 3):
+                for c in w_copy(n // 3):
                     c.wait()
-        with scope("slot"):
-            for s in range(2):
-                if p is not None:
-                    proj(p, s)
-                for n in posts:
-                    post(n, s)
         if k == 1:
             factors()
-        for n in posts:
-            if n % 3:
-                t, b = n // 3, n % 3 - 1
+        with scope("slot"):
+            for m in range(max(len(projs), len(posts))):
+                if m < len(projs):
+                    proj(*projs[m])
+                if m < len(posts):
+                    n, half = posts[m]
+                    post(n, half)
+                    if n % 3:
+                        contract(n // 3, half, n % 3 - 1)
+        for n, half in posts:
+            if n % 3 and half == 1:
                 for a in range(2):
-                    contract(t, a, b)
-                for a in range(2):
-                    send1(t, a, b)
-        if k == 3:
-            send_tails()
+                    send1(n // 3, a, n % 3 - 1)
         if k == 6:
             stage2(0)
         if k == 8:
@@ -389,9 +405,8 @@
             tail_copy(0).wait_recv()
 
     ext = jnp.concatenate(
-        [tail_rx[...].astype(F32), jnp.broadcast_to(xnew_ref[...].astype(F32), (8, D))], axis=0
+        [tail_rx[...].astype(F32), jnp.broadcast_to(xnew_ref[...].astype(F32), (12, D))], axis=0
     ).astype(BF)
-    a_own = i % 2
 
     def fresh(w, off, width):
         res = dot(ext, w)
@@ -399,7 +414,7 @@
         taps = cw_ref[:, cols] * 0.5
         acc = cb_ref[:, cols] * 0.5 + taps[3:4] * res[8:9]
         for k in range(3):
-            acc = acc + taps[k:k + 1] * jnp.where(a_own == 0, res[k:k + 1], res[3 + k:4 + k])
+            acc = acc + taps[k:k + 1] * res[k:k + 1]
         return acc + acc * jnp.tanh(acc)
 
     values = fresh(wx_ref[:, pl.ds(pl.multiple_of(j * 256, 256), 256)], j * 256, 256)
@@ -511,8 +526,9 @@
             pltpu.VMEM((G, 2 * T, 128), F32),
             pltpu.VMEM((G, 8, 256), F32),
             pltpu.VMEM((8, D), BF),
+            pltpu.VMEM((2, 4, D), BF),
             pltpu.VMEM((8, D), BF),
-            pltpu.VMEM((8, D), BF),
+            pltpu.VMEM((4, D), BF),
             pltpu.VMEM((2, 128), F32),
             pltpu.VMEM((SP, 2, 128), F32),
             pltpu.VMEM((16, N, 256), BF),

time: 41.1 us -> 38.4 us (0.934)
  the two profiles are of different devices: /device:TPU:27 before, /device:TPU:1 now
where the time goes in v4:
time: 38.4 us; the launch traced here: 38.3 us
  Pallas kernels  36.5 us (95%)
  local copies, waits for them, and re-layouts  1.19 us (3%)
  between operations  0.64 us (2%)
    pallas_call x1, Pallas kernels, per_device(): pl.pallas_call(kernel, out_shape=(pltpu.VMEM((1, R, P_SIZE, N), BF), pltp...  36.5 us
    unnamed x2, local copies, waits for them, and re-layouts  1.19 us

profile of v4, /device:TPU:1, one launch (start us, length us, event | category | flops | bytes accessed | tf_op | source)
XLA Modules:
  0.0 38.3 jit_solution(2650748236668122939)
XLA Ops:
  0.6 36.5 %shard_map.140 = (bf16[1,4,64,128]{3,2,1,0:T(8,128)(2,1)S(1)}, bf16[1,4,64]{2,1,0:T(4,128)(2,1)S(1)}) custom-call(bf16[2,384,2048]{2,1,0:T(8,128)(2,1)} %x_hbm.1, bf16[1,2048]{1,0:T(2,128)(2,1)} %xnew_hbm.1, bf16[2048,2048]{1,0:T(8,128)(2,1)} %wx_hbm.1, bf16[2048,1024]{1,0:T(8,128)(2,1)} %wb_hbm.1, bf16[2048,1024]{1,0:T(8,128)(2,1)} %wc_hbm.1, ...), custom_call_target="tpu_custom_call" | custom-call | tf_op jit(solution)/shard_map/pallas_call | solution.py:501
  37.1 0.6 %copy.17 = bf16[1,4,64,128]{3,2,1,0:T(8,128)(2,1)} copy(bf16[1,4,64,128]{3,2,1,0:T(8,128)(2,1)S(1)} %get-tuple-element.2) | data formatting | bytes 131072
  37.7 0.6 %copy.18 = bf16[1,4,64]{2,1,0:T(4,128)(2,1)} copy(bf16[1,4,64]{2,1,0:T(4,128)(2,1)S(1)} %get-tuple-element.3) | data formatting | bytes 1024

commit v5 on v4

--- a/solution.py
+++ b/solution.py
@@ -41,7 +41,7 @@
     x_hbm, xnew_hbm, wx_hbm, wb_hbm, wc_hbm, wdt_hbm, wz_hbm,
     cw_hbm, cb_hbm, dtb_hbm, alog_hbm, dskip_hbm, ng_hbm,
     st_out, ro_out,
-    x_ref, xnew_ref, wx_ref, wb_ref, wc_ref, wdt_ref, wz_ref,
+    x_ref, xnew_ref, w_ref, wc_ref, wdt_ref, wz_ref,
     cw_ref, cb_ref, dtb_ref, alog_ref, dskip_ref, ng_ref,
     pre_refs, key_refs, sc_refs, wg_ref, fac_ref,
     edge_tx, tail_tx, halo_rx, tail_rx, tot_tx, tot_rx,
@@ -83,8 +83,12 @@
         kcols = pl.ds(pl.multiple_of(q * 256, 256), 256)
         vcols = pl.ds(pl.multiple_of(q * 512, 512), 512)
         return [
-            pltpu.make_async_copy(wb_hbm.at[:, kcols], wb_ref.at[:, kcols], w_sems.at[t, 0]),
-            pltpu.make_async_copy(wx_hbm.at[:, vcols], wx_ref.at[:, vcols], w_sems.at[t, 1]),
+            pltpu.make_async_copy(
+                wb_hbm.at[:, kcols], w_ref.at[:, pl.ds(768 * t, 256)], w_sems.at[t, 0]
+            ),
+            pltpu.make_async_copy(
+                wx_hbm.at[:, vcols], w_ref.at[:, pl.ds(768 * t + 256, 512)], w_sems.at[t, 1]
+            ),
         ]
 
     for c in first_loads + w_copy(0):
@@ -183,20 +187,19 @@
         lax.broadcasted_iota(jnp.int32, (T, T), 1) > lax.broadcasted_iota(jnp.int32, (T, T), 0)
     ).astype(F32).astype(BF)
 
-    def weights(s):
-        own = steps[T * s:T * (s + 1)]
-        high = own.astype(BF)
-        low = (own - high.astype(F32)).astype(BF)
-        rest = dot(upper, high) + dot(upper, low)
-        weight = jnp.exp(rates * rest) * own
+    def rests():
+        parts = []
+        for s in range(2):
+            own = steps[T * s:T * (s + 1)]
+            high = own.astype(BF).astype(F32)
+            parts += [high, own - high]
+        res = dot(upper, jnp.concatenate(parts, axis=1).astype(BF))
+        return [res[:, 64 * s:64 * s + H] + res[:, 64 * s + H:64 * s + 2 * H] for s in range(2)]
+
+    def weights(s, rest):
+        weight = jnp.exp(rates * rest) * steps[T * s:T * (s + 1)]
         for g in range(G):
             wg_ref[g, T * s:T * (s + 1), 0:R] = weight[:, R * g:R * (g + 1)]
-
-    def w_slice(t, u):
-        q = pair(t)
-        if u == 0:
-            return wb_ref[:, pl.ds(pl.multiple_of(q * 256, 256), 256)]
-        return wx_ref[:, pl.ds(pl.multiple_of(q * 512 + 256 * (u - 1), 256), 256)]
 
     def put_halo(pre, rows):
         for c in range(2):
@@ -206,28 +209,33 @@
     def pre_of(n):
         return pre_refs[n % 6]
 
-    def proj(n, s):
-        pre = pre_of(n)
+    def proj(n, count, s):
         lead = 16 * (1 - s)
         start = (16 + T) * s
-        res = dot(x_ref[start:start + T + lead, :], w_slice(n // 3, n % 3))
-        for c in range(2):
-            pre[c, (T + 8) * s + 8:(T + 8) * (s + 1), :] = res[lead:lead + T, 128 * c:128 * (c + 1)]
-        if s == 0:
-            put_halo(pre, res[0:8])
-
-    with scope("w0wait"):
-        for c in w_copy(0) + conv_loads:
-            c.wait()
-
-    proj(0, 1)
+        wide = dot(x_ref[start:start + T + lead, :], w_ref[:, 256 * n:256 * (n + count)])
+        for k in range(count):
+            pre = pre_of(n + k)
+            res = wide[:, 256 * k:256 * (k + 1)]
+            for c in range(2):
+                pre[c, (T + 8) * s + 8:(T + 8) * (s + 1), :] = (
+                    res[lead:lead + T, 128 * c:128 * (c + 1)]
+                )
+            if s == 0:
+                put_halo(pre, res[0:8])
+
     for s in range(2):
         tot_tx[s:s + 1, 0:H] = jnp.sum(steps[T * s:T * (s + 1)], axis=0, keepdims=True)
     for d in range(1, SP):
         tot_copy(d).start()
-    proj(1, 1)
-    weights(0)
-    proj(2, 1)
+    with scope("w0wait"):
+        for c in w_copy(0) + conv_loads:
+            c.wait()
+
+    proj(0, 2, 1)
+    proj(2, 1, 1)
+    rest_sums = rests()
+    weights(0, rest_sums[0])
+    weights(1, rest_sums[1])
 
     with scope("halowait"):
         @pl.when(i > 0)
@@ -237,10 +245,8 @@
             c.wait()
     halo = jnp.where(i > 0, halo_rx[...].astype(F32), 0.0)
     x_ref[0:16, :] = jnp.concatenate([halo, jnp.zeros((8, D), F32)], axis=0).astype(BF)
-    proj(0, 0)
-    weights(1)
-    proj(1, 0)
-    proj(2, 0)
+    proj(0, 2, 0)
+    proj(2, 1, 0)
 
     lane = lax.broadcasted_iota(jnp.int32, (128, 128), 1)
 
@@ -294,10 +300,22 @@
         term = term * fac_ref[g, a:a + 1, :]
         tx1[4 * t + 2 * a + b] = term.astype(BF)
 
+    def s1_half(a, b, h):
+        n = 12 + 2 * a + b
+        cols = pl.ds(128 * h, 128)
+        return pltpu.make_async_remote_copy(
+            tx1.at[n, :, cols], rx1.at[3, xp, :, cols], s1_s.at[n + 4 * h], s1_r.at[3 + h, xp],
+            device_id=(zp * 4 + 2 * cp + a, 2 * yp + b), device_id_type=MESH,
+        )
+
+    def s1_sends(t, a, b):
+        return [s1_half(a, b, h) for h in range(2)] if t == 3 else [s1_copy(t, a, b)]
+
     def send1(t, a, b):
         @pl.when(jnp.logical_not(s1_own(a, b)))
         def _():
-            s1_copy(t, a, b).start()
+            for c in s1_sends(t, a, b):
+                c.start()
 
         @pl.when(s1_own(a, b))
         def _():
@@ -333,6 +351,31 @@
         else:
             s2_copy(t).start()
 
+    def s2_half(h):
+        cols = pl.ds(128 * h, 128)
+        return pltpu.make_async_remote_copy(
+            tx2.at[3, :, cols], rx2.at[zp, :, cols], s2_s.at[3 + h], s2_r.at[zp],
+            device_id=(yp * 4 + xp, 2 * pair(3) + cp), device_id_type=MESH,
+        )
+
+    def stage2_last():
+        for h in range(2):
+            cols = pl.ds(128 * h, 128)
+            with scope("s1wait"):
+                for d in range(4):
+                    @pl.when(jnp.logical_not((d == xp) & s1_self))
+                    def _():
+                        pltpu.make_async_remote_copy(
+                            tx1.at[0, :, cols], rx1.at[3, d, :, cols],
+                            s1_s.at[0], s1_r.at[3 + h, d],
+                            device_id=(i, j), device_id_type=MESH,
+                        ).wait_recv()
+            acc = rx1[3, 0, :, cols].astype(F32)
+            for d in range(1, 4):
+                acc = acc + rx1[3, d, :, cols].astype(F32)
+            tx2[3, :, cols] = acc.astype(BF)
+            s2_half(h).start()
+
     def factors():
         with scope("totwait"):
             for d in range(1, SP):
@@ -345,18 +388,18 @@
         for d in range(SP):
             later = later + jnp.where(i < d, tot_rx[d], 0.0)
         factor = jnp.exp(rates * later[:, 0:H])
-        spread = (
-            lax.broadcasted_iota(jnp.int32, (H, H * P_SIZE), 1) // P_SIZE
-            == lax.broadcasted_iota(jnp.int32, (H, H * P_SIZE), 0)
-        ).astype(F32)
-        wide = dot_exact(jnp.concatenate([factor, jnp.zeros((6, H), F32)], axis=0), spread)
+        first = lax.broadcasted_iota(jnp.int32, (2, 128), 1) < P_SIZE
         for g in range(G):
-            fac_ref[g] = wide[:, 256 * g:256 * (g + 1)]
+            for c in range(2):
+                h = R * g + 2 * c
+                fac_ref[g, 0:2, 128 * c:128 * (c + 1)] = jnp.where(
+                    first, factor[:, h:h + 1], factor[:, h + 1:h + 2]
+                )
 
     slots = (
-        ("3a3b", "0a0b"), ("4a4b", "1a1b"), ("5a5b", "2a2b3a"), ("6a6b", "3b4a4b"),
-        ("7a7b", "5a5b6a"), ("8a8b", "6b7a7b"), ("9a9b", "8a8b9a"), ("10a10b", "9b10a"),
-        ("11a", "10b"), ("11b", "11a11b"),
+        ((3, 2, 0), "0a0b"), ((3, 2, 1), "1a1b"), ((5, 2, 0), "2a2b3a"), ((5, 2, 1), "3b4a4b"),
+        ((7, 2, 0), "5a5b6a"), ((7, 2, 1), "6b7a"), ((9, 2, 0), "7b8a8b"), ((9, 2, 1), "9a9b"),
+        ((11, 1, 0), "10a10b"), ((11, 1, 1), "11a"), (None, "11b"),
     )
 
     def halves(text):
@@ -369,28 +412,24 @@
                 num += ch
         return out
 
-    for k, (projs, posts) in enumerate(slots):
-        projs, posts = halves(projs), halves(posts)
-        n = projs[0][0]
-        if projs[0][1] == 0 and n % 3 == 0 and n > 3:
+    for k, (project_unit, posts) in enumerate(slots):
+        posts = halves(posts)
+        if k in (2, 6):
             with scope("wwait"):
-                for c in w_copy(n // 3):
+                for c in w_copy(2 if k == 2 else 3):
                     c.wait()
         if k == 1:
             factors()
         with scope("slot"):
-            for m in range(max(len(projs), len(posts))):
-                if m < len(projs):
-                    proj(*projs[m])
-                if m < len(posts):
-                    n, half = posts[m]
-                    post(n, half)
-                    if n % 3:
-                        contract(n // 3, half, n % 3 - 1)
+            if project_unit is not None:
+                proj(*project_unit)
+            for n, half in posts:
+                post(n, half)
+                if n % 3:
+                    contract(n // 3, half, n % 3 - 1)
         for n, half in posts:
-            if n % 3 and half == 1:
-                for a in range(2):
-                    send1(n // 3, a, n % 3 - 1)
+            if n % 3:
+                send1(n // 3, half, n % 3 - 1)
         if k == 6:
             stage2(0)
         if k == 8:
@@ -417,8 +456,12 @@
             acc = acc + taps[k:k + 1] * res[k:k + 1]
         return acc + acc * jnp.tanh(acc)
 
-    values = fresh(wx_ref[:, pl.ds(pl.multiple_of(j * 256, 256), 256)], j * 256, 256)
-    keys = fresh(wb_ref[:, pl.ds(pl.multiple_of(j * N, N), N)], H * P_SIZE + j * N, N)
+    turn = (zp + 4 - yp) % 4
+    place = 768 * (turn + (turn // 2) * (1 - 2 * (turn % 2)))
+    vcols = pl.ds(pl.multiple_of(place + 256 + 256 * cp, 256), 256)
+    kcols = pl.ds(pl.multiple_of(place + N * cp, N), N)
+    values = fresh(w_ref[:, vcols], j * 256, 256)
+    keys = fresh(w_ref[:, kcols], H * P_SIZE + j * N, N)
     query = fresh(wc_ref[...], H * P_SIZE + G * N + j * N, N)
     gate = dot(ext, wz_ref[...])[8:9]
     new_raw = dot_t(ext, wdt_ref[...])[8:9]
@@ -438,7 +481,7 @@
     gate = gate * jax.nn.sigmoid(gate)
 
     stage2(2)
-    stage2(3)
+    stage2_last()
 
     with scope("s2wait"):
         for d in range(4):
@@ -483,11 +526,15 @@
                 for b in range(2):
                     @pl.when(jnp.logical_not(s1_own(a, b)))
                     def _():
-                        s1_copy(t, a, b).wait_send()
+                        for c in s1_sends(t, a, b):
+                            c.wait_send()
             if OFFS[t] == 0:
                 @pl.when(yp != zp)
                 def _():
                     s2_copy(t).wait_send()
+            elif t == 3:
+                for h in range(2):
+                    s2_half(h).wait_send()
             else:
                 s2_copy(t).wait_send()
 
@@ -509,8 +556,7 @@
         scratch_shapes=[
             pltpu.VMEM((2 * T + 16, D), BF),
             pltpu.VMEM((1, D), BF),
-            pltpu.VMEM((D, H * P_SIZE), BF),
-            pltpu.VMEM((D, G * N), BF),
+            pltpu.VMEM((D, H * P_SIZE + G * N), BF),
             pltpu.VMEM((D, N), BF),
             pltpu.VMEM((H, D), BF),
             pltpu.VMEM((D, 256), BF),
@@ -543,9 +589,9 @@
             dma,
             dma((SP,)),
             dma((SP,)),
-            dma((16,)),
-            dma((4, 4)),
-            dma((4,)),
+            dma((20,)),
+            dma((5, 4)),
+            dma((5,)),
             dma((4,)),
         ],
         compiler_params=pltpu.CompilerParams(

time: 38.4 us -> 35.8 us (0.932)
  Pallas kernels: 36.5 us -> 33.8 us
    pallas_call x1, Pallas kernels: 36.5 us -> 33.8 us  [per_device(): pl.pallas_call(kernel, out_shape=(pltpu.VMEM((1, R, P_SIZE, N), BF), pltp...]
where the time goes in v5:
time: 35.8 us; the launch traced here: 35.7 us
  Pallas kernels  33.8 us (94%)
  local copies, waits for them, and re-layouts  1.19 us (3%)
  between operations  0.64 us (2%)
    pallas_call x1, Pallas kernels, per_device(): pl.pallas_call(kernel, out_shape=(pltpu.VMEM((1, R, P_SIZE, N), BF), pltp...  33.8 us
    unnamed x2, local copies, waits for them, and re-layouts  1.19 us

profile of v5, /device:TPU:1, one launch (start us, length us, event | category | flops | bytes accessed | tf_op | source)
XLA Modules:
  0.0 35.7 jit_solution(12667521637602529905)
XLA Ops:
  0.6 33.8 %shard_map.140 = (bf16[1,4,64,128]{3,2,1,0:T(8,128)(2,1)S(1)}, bf16[1,4,64]{2,1,0:T(4,128)(2,1)S(1)}) custom-call(bf16[2,384,2048]{2,1,0:T(8,128)(2,1)} %x_hbm.1, bf16[1,2048]{1,0:T(2,128)(2,1)} %xnew_hbm.1, bf16[2048,2048]{1,0:T(8,128)(2,1)} %wx_hbm.1, bf16[2048,1024]{1,0:T(8,128)(2,1)} %wb_hbm.1, bf16[2048,1024]{1,0:T(8,128)(2,1)} %wc_hbm.1, ...), custom_call_target="tpu_custom_call" | custom-call | tf_op jit(solution)/shard_map/pallas_call | solution.py:548
  34.5 0.6 %copy.17 = bf16[1,4,64,128]{3,2,1,0:T(8,128)(2,1)} copy(bf16[1,4,64,128]{3,2,1,0:T(8,128)(2,1)S(1)} %get-tuple-element.2) | data formatting | bytes 131072
  35.1 0.6 %copy.18 = bf16[1,4,64]{2,1,0:T(4,128)(2,1)} copy(bf16[1,4,64]{2,1,0:T(4,128)(2,1)S(1)} %get-tuple-element.3) | data formatting | bytes 1024

commit v6 on v5

--- a/solution.py
+++ b/solution.py
@@ -150,28 +150,6 @@
     def _():
         halo_copy.start()
 
-    def tail_copy(n):
-        return pltpu.make_async_remote_copy(
-            tail_tx.at[n % 2], tail_rx, tail_s.at[n], tail_r,
-            device_id=(2 * j + n % 2, n // 2), device_id_type=MESH,
-        )
-
-    def tail_self(n):
-        return (j == 7) & (2 * j + n % 2 == i) & (n // 2 == j)
-
-    @pl.when(i == SP - 1)
-    def _():
-        tail_tx[0] = jnp.concatenate([lo, lo[0:1]], axis=0).astype(BF)
-        tail_tx[1] = jnp.concatenate([hi, hi[0:1]], axis=0).astype(BF)
-        for n in range(16):
-            @pl.when(jnp.logical_not(tail_self(n)))
-            def _():
-                tail_copy(n).start()
-
-    @pl.when((i == SP - 1) & (j == 7))
-    def _():
-        tail_rx[...] = tail_tx[1]
-
     raw = jnp.concatenate([raw0, dot_t(x_ref[16 + T:16 + 2 * T, :], wdt_ref[...])], axis=0)
     steps = softplus(raw + dtb_ref[...])
     tot_tx[...] = jnp.zeros_like(tot_tx)
@@ -227,6 +205,28 @@
         tot_tx[s:s + 1, 0:H] = jnp.sum(steps[T * s:T * (s + 1)], axis=0, keepdims=True)
     for d in range(1, SP):
         tot_copy(d).start()
+    def tail_copy(n):
+        return pltpu.make_async_remote_copy(
+            tail_tx.at[n % 2], tail_rx, tail_s.at[n], tail_r,
+            device_id=(2 * j + n % 2, n // 2), device_id_type=MESH,
+        )
+
+    def tail_self(n):
+        return (j == 7) & (2 * j + n % 2 == i) & (n // 2 == j)
+
+    @pl.when(i == SP - 1)
+    def _():
+        tail_tx[0] = jnp.concatenate([lo, lo[0:1]], axis=0).astype(BF)
+        tail_tx[1] = jnp.concatenate([hi, hi[0:1]], axis=0).astype(BF)
+        for n in range(16):
+            @pl.when(jnp.logical_not(tail_self(n)))
+            def _():
+                tail_copy(n).start()
+
+    @pl.when((i == SP - 1) & (j == 7))
+    def _():
+        tail_rx[...] = tail_tx[1]
+
     with scope("w0wait"):
         for c in w_copy(0) + conv_loads:
             c.wait()

time: 35.8 us -> 35.8 us (level)
  no operation moved by 1% of the time
where the time goes in v6:
time: 35.8 us; the launch traced here: 35.7 us
  Pallas kernels  33.8 us (94%)
  local copies, waits for them, and re-layouts  1.19 us (3%)
  between operations  0.64 us (2%)
    pallas_call x1, Pallas kernels, per_device(): pl.pallas_call(kernel, out_shape=(pltpu.VMEM((1, R, P_SIZE, N), BF), pltp...  33.8 us
    unnamed x2, local copies, waits for them, and re-layouts  1.19 us

profile of v6, /device:TPU:1, one launch (start us, length us, event | category | flops | bytes accessed | tf_op | source)
XLA Modules:
  0.0 35.7 jit_solution(219575889692005536)
XLA Ops:
  0.6 33.8 %shard_map.140 = (bf16[1,4,64,128]{3,2,1,0:T(8,128)(2,1)S(1)}, bf16[1,4,64]{2,1,0:T(4,128)(2,1)S(1)}) custom-call(bf16[2,384,2048]{2,1,0:T(8,128)(2,1)} %x_hbm.1, bf16[1,2048]{1,0:T(2,128)(2,1)} %xnew_hbm.1, bf16[2048,2048]{1,0:T(8,128)(2,1)} %wx_hbm.1, bf16[2048,1024]{1,0:T(8,128)(2,1)} %wb_hbm.1, bf16[2048,1024]{1,0:T(8,128)(2,1)} %wc_hbm.1, ...), custom_call_target="tpu_custom_call" | custom-call | tf_op jit(solution)/shard_map/pallas_call | solution.py:548
  34.5 0.6 %copy.17 = bf16[1,4,64,128]{3,2,1,0:T(8,128)(2,1)} copy(bf16[1,4,64,128]{3,2,1,0:T(8,128)(2,1)S(1)} %get-tuple-element.2) | data formatting | bytes 131072
  35.1 0.6 %copy.18 = bf16[1,4,64]{2,1,0:T(4,128)(2,1)} copy(bf16[1,4,64]{2,1,0:T(4,128)(2,1)S(1)} %get-tuple-element.3) | data formatting | bytes 1024
